TPU v7x, 512 devices: a 8x2x16 block of a 8x8x16 slice. The times are simulated.
512 devices in a mesh: grp: 2 (over y), dp: 8 (over x), kv: 16 (over z), tp: 2 (over core).
Axes of the slice: x: 8, y: 2, z: 16, core: 2. Of those that a mesh axis runs over, the one named last changes fastest.
The devices are a block of a 8x8x16 slice.
Arguments:
- candidate_vectors: bfloat16 [512, 4, 2048], P(('grp', 'dp'), None, ('kv', 'tp')), parts along dimension 0, may hold values from -6 to 6
- leading_scaling_factor: bfloat16 [2048], replicated, may hold values from 0.099609375 to 1.8984375
- lane_feed_matrix: bfloat16 [2048, 32, 2, 64], P(None, 'kv', 'tp')
- final_valve_matrix: bfloat16 [2048, 32, 2, 64], P(None, 'kv', 'tp'), may hold values from -0.125 to 0.125
- increment_matrix: bfloat16 [2048, 32, 2], replicated, may hold values from -0.125 to 0.125
- entry_basis_matrix: bfloat16 [2048, 2, 128], P(None, 'tp'), may hold values from -0.125 to 0.125
- readout_basis_matrix: bfloat16 [2048, 2, 128], P(None, 'tp'), may hold values from -0.125 to 0.125
- lane_feed_kernel: float32 [4, 32, 2, 64], P(None, 'kv', 'tp'), may hold values from -3 to 3
- entry_basis_kernel: float32 [4, 2, 128], P(None, 'tp'), may hold values from -3 to 3
- readout_basis_kernel: float32 [4, 2, 128], P(None, 'tp'), may hold values from -3 to 3
- increment_offset: float32 [32, 2], P('kv', 'tp'), may hold values from -4 to 1
- shrink_speed_exponent: float32 [32, 2], P('kv', 'tp'), may hold values from 0 to 2.8
- lane_bypass_factor: float32 [32, 2], P('kv', 'tp'), may hold values from 0.5 to 1.5
- final_linear_matrix: bfloat16 [32, 2, 64, 2048], P(None, None, None, ('kv', 'tp')), may hold values from -0.09375 to 0.09375
- hidden_carried_memory: float32 [512, 32, 2, 64, 128], P(('grp', 'dp'), 'kv', 'tp'), parts along dimension 0, may hold values from -0.6 to 0.6
- lane_filter_memory: bfloat16 [512, 7, 32, 2, 64], P(('grp', 'dp'), None, 'kv', 'tp'), parts along dimension 0, may hold values from -6 to 6
- entry_basis_memory: bfloat16 [512, 7, 2, 128], P(('grp', 'dp'), None, 'tp'), parts along dimension 0, may hold values from -6 to 6
- readout_basis_memory: bfloat16 [512, 7, 2, 128], P(('grp', 'dp'), None, 'tp'), parts along dimension 0, may hold values from -6 to 6
- predecessor_index: int32 [512, 4], P(('grp', 'dp')), parts along dimension 0, may hold values from -1 to 2, as said below
- admitted_counts: int32 [512], P(('grp', 'dp')), parts along dimension 0, may hold values from 0 to 4
- surplus_fading: float32 [512, 4, 32, 2], P(('grp', 'dp'), None, 'kv', 'tp'), parts along dimension 0, may hold values from -0.7 to 0, as said below
Outputs:
- mixed: bfloat16 [512, 4, 2048], P(('grp', 'dp'), None, ('kv', 'tp')), parts along dimension 0
There are 2 independent parts, one for each index of `grp`. A program takes and returns all parts, laid end to end along the dimension named above; an argument that names none is the same for every part. Nothing has to cross between parts.
Inputs may be any that keep to these rules, and one draw needn't show every extreme that they name: predecessor_index[s, j] is -1 or a smaller proposal index than j. `surplus_fading`: zero except at a few proposals and heads.
All inputs are finite; a program needn't handle non-finite values.
Results may differ from a plain program's by a relative error of at most 0.012.
Values may be sent and summed in bfloat16 or wider, within the bound.
No kernel may reach another device: no remote copies, remote signals or barrier semaphores. Data moves between devices by JAX's collectives and lax.ppermute only.
A program may use at most 64 MiB of HBM per device.

v0:
```python
import jax
import jax.numpy as jnp
from jax import lax
from jax.sharding import PartitionSpec as P

D = 2048
HG = 32
G = 2
HD = 64
N = 128
CONV = 4
WIN = 7


def laid_out(pieces, dim):
    pieces = jnp.moveaxis(pieces, 0, dim)
    lengths = pieces.shape
    return pieces.reshape(*lengths[:dim], lengths[dim] * lengths[dim + 1], *lengths[dim + 2 :])


def from_everyone(x, axis):
    copies = jnp.broadcast_to(x, (lax.axis_size(axis), *x.shape))
    return lax.all_to_all(copies, axis, split_axis=0, concat_axis=0, tiled=True)


def gathered_copies(x, axis, dim):
    return laid_out(from_everyone(x, axis), dim)


def lineage_tables(predecessor_index):
    seqs, props = predecessor_index.shape
    column = jnp.arange(props, dtype=jnp.int32)
    current = jnp.broadcast_to(column[None, :], (seqs, props))
    depth = jnp.zeros((seqs, props), jnp.int32)
    onehots = []
    for step in range(props):
        onehots.append((current[:, :, None] == column[None, None, :]).astype(jnp.float32))
        if step > 0:
            depth = depth + (current >= 0).astype(jnp.int32)
        upward = jnp.take_along_axis(predecessor_index, jnp.maximum(current, 0), axis=1)
        current = jnp.where(current >= 0, upward, -1)
    return (onehots, depth)


def conv_tree(current, saved, taps, onehots, depth, admitted_counts):
    slots = jnp.arange(saved.shape[1], dtype=jnp.int32)
    cur_f = current.astype(jnp.float32)
    saved_f = saved.astype(jnp.float32)
    total = jnp.zeros(cur_f.shape, jnp.float32)
    for lag in range(CONV):
        value = jnp.einsum("sji,sic->sjc", onehots[lag], cur_f)
        target = admitted_counts[:, None] + (CONV - 1) - (lag - depth)
        chosen = ((depth < lag)[:, :, None] & (slots[None, None, :] == target[:, :, None])).astype(
            jnp.float32
        )
        value = value + jnp.einsum("sjw,swc->sjc", chosen, saved_f)
        total = total + taps[CONV - 1 - lag] * value
    return jax.nn.silu(total)


def shards(
    candidate_vectors,
    leading_scaling_factor,
    lane_feed_matrix,
    final_valve_matrix,
    increment_matrix,
    entry_basis_matrix,
    readout_basis_matrix,
    lane_feed_kernel,
    entry_basis_kernel,
    readout_basis_kernel,
    increment_offset,
    shrink_speed_exponent,
    lane_bypass_factor,
    final_linear_matrix,
    hidden_carried_memory,
    lane_filter_memory,
    entry_basis_memory,
    readout_basis_memory,
    predecessor_index,
    admitted_counts,
    surplus_fading,
):
    seqs, props, feat_dev = candidate_vectors.shape
    heads_dev = increment_offset.shape[0]
    rows = seqs * props
    kv_index = lax.axis_index("kv")
    tp_index = lax.axis_index("tp")
    dt_own = lax.dynamic_slice(
        increment_matrix, (0, kv_index * heads_dev, tp_index), (D, heads_dev, 1)
    ).reshape(D, heads_dev)
    wx_flat = lane_feed_matrix.reshape(D, heads_dev * HD)
    wz_flat = final_valve_matrix.reshape(D, heads_dev * HD)
    wb_flat = entry_basis_matrix.reshape(D, N)
    wc_flat = readout_basis_matrix.reshape(D, N)
    piece = gathered_copies(candidate_vectors, ("kv", "tp"), 2)
    width = piece.shape[2]
    piece_f = piece.astype(jnp.float32)
    gain = leading_scaling_factor.astype(jnp.float32)
    scaled = (piece_f * gain).astype(jnp.bfloat16).reshape(rows, width)

    def partial_dot(source, weight):
        return jnp.dot(source, weight, preferred_element_type=jnp.float32)

    x_acc = partial_dot(scaled, wx_flat)
    z_acc = partial_dot(scaled, wz_flat)
    dt_acc = partial_dot(scaled, dt_own)
    b_acc = partial_dot(scaled, wb_flat)
    c_acc = partial_dot(scaled, wc_flat)
    squares = jnp.sum(piece_f * piece_f, axis=2).reshape(rows)
    r_in = lax.rsqrt(squares / D + 1e-06)
    x_rows = (x_acc * r_in[:, None]).astype(jnp.bfloat16).reshape(seqs, props, heads_dev * HD)
    z_rows = (z_acc * r_in[:, None]).astype(jnp.bfloat16).reshape(seqs, props, heads_dev, 1, HD)
    dt_raw = (dt_acc * r_in[:, None]).reshape(seqs, props, heads_dev, 1)
    b_flat = (b_acc * r_in[:, None]).astype(jnp.bfloat16)
    c_flat = (c_acc * r_in[:, None]).astype(jnp.bfloat16)
    onehots, depth = lineage_tables(predecessor_index)
    x_conv = conv_tree(
        x_rows,
        lane_filter_memory.reshape(seqs, WIN, -1),
        lane_feed_kernel.reshape(CONV, -1),
        onehots,
        depth,
        admitted_counts,
    ).reshape(seqs, props, heads_dev, 1, HD)
    b_conv = conv_tree(
        b_flat.reshape(seqs, props, N),
        entry_basis_memory.reshape(seqs, WIN, N),
        entry_basis_kernel.reshape(CONV, N),
        onehots,
        depth,
        admitted_counts,
    ).reshape(seqs, props, 1, N)
    c_conv = conv_tree(
        c_flat.reshape(seqs, props, N),
        readout_basis_memory.reshape(seqs, WIN, N),
        readout_basis_kernel.reshape(CONV, N),
        onehots,
        depth,
        admitted_counts,
    ).reshape(seqs, props, 1, N)
    lineage = sum(onehots)
    lane_increment = jax.nn.softplus(dt_raw + increment_offset)
    fading_exponent = -jnp.exp(shrink_speed_exponent) * lane_increment + surplus_fading
    level = jnp.einsum("sji,sihg->sjhg", lineage, fading_exponent)
    gap = level[:, :, None] - level[:, None, :]
    weight = jnp.where(lineage[:, :, :, None, None] > 0, jnp.exp(jnp.minimum(gap, 0.0)), 0.0)
    scores = jnp.einsum("sjgn,sign->sjig", c_conv, b_conv)
    mixing = weight * scores[:, :, :, None, :] * lane_increment[:, None]
    y_rows = jnp.einsum("sjihg,sihgp->sjhgp", mixing, x_conv)
    y_rows = y_rows + jnp.exp(level)[..., None] * jnp.einsum(
        "shgpn,sjgn->sjhgp", hidden_carried_memory, c_conv
    )
    y_rows = y_rows + lane_bypass_factor[..., None] * x_conv
    gated = (
        (y_rows * jax.nn.silu(z_rows.astype(jnp.float32)))
        .astype(jnp.bfloat16)
        .reshape(rows, heads_dev * HD)
    )
    kv_count = lax.axis_size("kv")
    out_cols = final_linear_matrix.shape[3]
    out_flat = jnp.transpose(
        final_linear_matrix.reshape(kv_count, heads_dev, G, HD, out_cols), (0, 2, 1, 3, 4)
    ).reshape(HG * G * HD, out_cols)
    piece = gathered_copies(gated, ("kv", "tp"), 1)
    piece_f = piece.astype(jnp.float32)
    product = jnp.dot(piece, out_flat, preferred_element_type=jnp.float32)
    sumsq = jnp.sum(piece_f * piece_f, axis=1)
    r_out = lax.rsqrt(sumsq / (HG * G * HD) + 1e-05)
    return (product * r_out[:, None]).astype(jnp.bfloat16).reshape(seqs, props, out_cols)


def solution(mesh):
    placed = (
        P(("grp", "dp"), None, ("kv", "tp")),
        P(),
        P(None, "kv", "tp", None),
        P(None, "kv", "tp", None),
        P(),
        P(None, "tp", None),
        P(None, "tp", None),
        P(None, "kv", "tp", None),
        P(None, "tp", None),
        P(None, "tp", None),
        P("kv", "tp"),
        P("kv", "tp"),
        P("kv", "tp"),
        P(None, None, None, ("kv", "tp")),
        P(("grp", "dp"), "kv", "tp", None, None),
        P(("grp", "dp"), None, "kv", "tp", None),
        P(("grp", "dp"), None, "tp", None),
        P(("grp", "dp"), None, "tp", None),
        P(("grp", "dp"), None),
        P(("grp", "dp")),
        P(("grp", "dp"), None, "kv", "tp"),
    )
    return jax.shard_map(
        shards,
        mesh=mesh,
        in_specs=placed,
        out_specs=P(("grp", "dp"), None, ("kv", "tp")),
        check_vma=False,
    )
```

profile of v0, /device:TPU:65, one launch (start us, length us, event | category | flops | bytes accessed | tf_op | source)
XLA Modules:
  0.0 178.1 jit_solution(1571273258071741870)
XLA Ops:
  0.0 1.4 broadcast_in_dim.21
  1.4 1.6 reshape.449
  3.0 45.2 %all-to-all-start = ((bf16[32,2,4096]{2,1,0:T(2,128)(2,1)}), bf16[32,2,4096]{2,1,0:T(2,128)(2,1)S(1)}, u32[]{:S(2)}, u32[]{:S(2)}) async-start(bf16[32,2,4096]{2,1,0:T(2,128)(2,1)} %reshape.449), calls=%async_computation | async-start | bytes 1048576 | tf_op jit(solution)/shard_map/all_to_all | solution.py:23
  48.5 1.5 gather_fusion
  50.5 1.5 gather_fusion.1
  52.5 1.5 gather_fusion.2
  56.0 0.5 negate_bitcast_fusion
  56.5 0.6 slice_bitcast_fusion.4
  57.1 0.6 slice_bitcast_fusion
  57.7 0.7 constant_dynamic-slice_fusion
  58.4 0.8 fusion.81
  59.2 22.4 %all-to-all-done = bf16[32,2,4096]{2,1,0:T(2,128)(2,1)S(1)} async-done(((bf16[32,2,4096]{2,1,0:T(2,128)(2,1)}), bf16[32,2,4096]{2,1,0:T(2,128)(2,1)S(1)}, u32[]{:S(2)}, u32[]{:S(2)}) %all-to-all-start) | async-done | bytes 524320 | tf_op jit(solution)/shard_map/all_to_all | solution.py:23
  81.6 1.7 reshape.450
  83.3 2.4 %fusion.1 = (f32[32,4]{1,0:T(8,128)S(1)}, bf16[32,4,32,64]{3,1,0,2:T(4,128)(2,1)S(1)}) fusion(bf16[32,32,4,64]{3,2,1,0:T(4,128)(2,1)} %reshape.450, f32[32,64]{1,0:T(8,128)S(1)} %reshape.374), kind=kLoop, calls=%fused_computation.6 | loop fusion | flops 1310592 | bytes 1057280 | tf_op jit(solution)/shard_map/reduce_sum | solution.py:110
  85.8 2.2 %copy.151 = bf16[32,4,32,64]{3,2,1,0:T(8,128)(2,1)} copy(bf16[32,4,32,64]{3,1,0,2:T(4,128)(2,1)S(1)} %get-tuple-element.17) | data formatting | bytes 1048576 | tf_op jit(solution)/shard_map/convert_element_type | solution.py:100
  88.0 2.3 %convert_element_type.120 = bf16[128,2048]{1,0:T(8,128)(2,1)S(1)} reshape(bf16[32,4,32,64]{3,2,1,0:T(8,128)(2,1)} %copy.151) | data formatting | bytes 1048576 | tf_op jit(solution)/shard_map/convert_element_type | solution.py:100
  90.3 0.2 convolution_multiply_fusion.5
  90.6 0.1 reshape.363
  90.8 0.3 fusion.25
  91.1 0.2 fusion.56
  91.4 0.2 fusion.59
  91.6 0.2 fusion.62
  91.8 0.2 fusion.65
  92.0 0.3 fusion.24
  92.3 0.3 fusion.23
  92.6 0.3 fusion.21
  92.8 0.3 divide_multiply_fusion.2
  93.1 0.7 reshape.353
  93.9 0.1 reshape.426
  94.0 1.4 fusion.26
  95.4 0.8 fusion.55
  96.3 0.9 fusion.58
  97.1 1.3 fusion.27
  98.4 0.9 fusion.54
  99.3 0.9 fusion.57
  100.2 0.9 fusion.61
  101.0 0.8 fusion.64
  101.8 0.9 fusion.60
  102.7 0.1 fusion.63
  102.8 0.8 compare_select_fusion
  103.6 0.6 copy.185
  104.2 0.3 fusion.29
  104.8 0.3 fusion.119
  105.2 0.1 reshape.375
  105.3 1.1 fusion.17
  106.4 1.1 fusion.16
  107.6 1.1 fusion.14
  108.7 1.1 fusion.10
  109.8 1.1 fusion.9
  111.0 0.3 fusion.7
  111.3 0.3 divide_multiply_fusion
  111.6 0.4 convolution_bitcast_fusion
  112.0 0.3 copy.184
  112.3 0.9 fusion.2
  113.3 0.3 fusion.37
  113.6 0.1 fusion.36
  114.0 1.2 broadcast_in_dim.25
  115.2 4.6 %all-to-all-start.1 = ((bf16[32,128,128]{1,2,0:T(8,128)(2,1)}), bf16[32,128,128]{1,2,0:T(8,128)(2,1)S(1)}, u32[]{:S(2)}, u32[]{:S(2)}) async-start(bf16[32,128,128]{1,2,0:T(8,128)(2,1)} %broadcast_in_dim.25), calls=%async_computation.1 | async-start | bytes 2097152 | tf_op jit(solution)/shard_map/all_to_all | solution.py:23
  119.8 3.9 %copy.196 = bf16[16,2,2,64,64]{3,1,2,0,4:T(2,128)(2,1)} copy(bf16[16,2,2,64,64]{4,3,2,1,0:T(8,128)(2,1)} %bitcast.134) | data formatting | bytes 1048576 | tf_op jit(solution)/shard_map/reshape | solution.py:163
  123.7 3.9 %reshape.370 = bf16[4096,64]{0,1:T(8,128)(2,1)} reshape(bf16[16,2,2,64,64]{3,2,1,0,4:T(2,128)(2,1)} %bitcast.133) | data formatting | bytes 1048576 | tf_op jit(solution)/shard_map/reshape | solution.py:164
  127.6 47.9 %all-to-all-done.1 = bf16[32,128,128]{1,2,0:T(8,128)(2,1)S(1)} async-done(((bf16[32,128,128]{1,2,0:T(8,128)(2,1)}), bf16[32,128,128]{1,2,0:T(8,128)(2,1)S(1)}, u32[]{:S(2)}, u32[]{:S(2)}) %all-to-all-start.1) | async-done | bytes 1048608 | tf_op jit(solution)/shard_map/all_to_all | solution.py:23
  175.4 0.6 multiply_reduce_fusion
  176.0 1.4 fusion.30
  177.4 0.7 copy.197
  (130 shorter events, 3.9 us)
Async XLA Ops:
  0.0 112.3 %copy-start = (f32[32,2,1,64,128]{4,3,2,1,0:T(8,128)S(1)}, f32[32,2,1,64,128]{4,3,2,1,0:T(8,128)}, u32[]{:S(2)}) copy-start(f32[32,2,1,64,128]{4,3,2,1,0:T(8,128)} %param.37) | copy-start | bytes 6291460
  0.0 48.5 %copy-start.1 = (s32[32,4]{0,1:T(4,128)S(1)}, s32[32,4]{0,1:T(4,128)}, u32[]{:S(2)}) copy-start(s32[32,4]{0,1:T(4,128)} %param.41) | copy-start | bytes 1540
  3.0 78.6 %all-to-all-start = ((bf16[32,2,4096]{2,1,0:T(2,128)(2,1)}), bf16[32,2,4096]{2,1,0:T(2,128)(2,1)S(1)}, u32[]{:S(2)}, u32[]{:S(2)}) async-start(bf16[32,2,4096]{2,1,0:T(2,128)(2,1)} %reshape.449), calls=%async_computation | async-start | bytes 1048576 | tf_op jit(solution)/shard_map/all_to_all | solution.py:23
  52.4 1.8 %copy-start.24 = (f32[4,2,1,64]{3,2,1,0:T(1,128)S(1)}, f32[4,2,1,64]{3,2,1,0:T(1,128)}, u32[]{:S(2)}) copy-start(f32[4,2,1,64]{3,2,1,0:T(1,128)} %param.30) | copy-start | bytes 6148
  52.4 2.9 %copy-start.35 = (s32[32]{0:T(128)S(1)}, s32[32]{0:T(128)}, u32[]{:S(2)}) copy-start(s32[32]{0:T(128)} %param.42) | copy-start | bytes 388
  52.4 3.2 %copy-start.16 = (bf16[2048]{0:T(1024)(128)(2,1)S(1)}, bf16[2048]{0:T(1024)(128)(2,1)}, u32[]{:S(2)}) copy-start(bf16[2048]{0:T(1024)(128)(2,1)} %param.24) | copy-start | bytes 12292
  52.4 3.3 %copy-start.17 = (f32[32,4,2,1]{0,3,2,1:T(1,128)S(1)}, f32[32,4,2,1]{0,3,2,1:T(1,128)}, u32[]{:S(2)}) copy-start(f32[32,4,2,1]{0,3,2,1:T(1,128)} %param.43) | copy-start | bytes 3076
  52.4 3.4 %copy-start.4 = (bf16[32,7,2,1,64]{4,2,3,1,0:T(2,128)(2,1)S(1)}, bf16[32,7,2,1,64]{4,2,3,1,0:T(2,128)(2,1)}, u32[]{:S(2)}) copy-start(bf16[32,7,2,1,64]{4,2,3,1,0:T(2,128)(2,1)} %param.38) | copy-start | bytes 172036
  52.4 3.5 %copy-start.36 = (f32[2,1]{0,1:T(1,128)S(1)}, f32[2,1]{0,1:T(1,128)}, u32[]{:S(2)}) copy-start(f32[2,1]{0,1:T(1,128)} %param.34) | copy-start | bytes 28
  52.5 4.0 %copy-start.25 = (f32[4,1,128]{2,1,0:T(1,128)S(1)}, f32[4,1,128]{2,1,0:T(1,128)}, u32[]{:S(2)}) copy-start(f32[4,1,128]{2,1,0:T(1,128)} %param.31) | copy-start | bytes 6148
  52.5 4.6 %copy-start.26 = (f32[4,1,128]{2,1,0:T(1,128)S(1)}, f32[4,1,128]{2,1,0:T(1,128)}, u32[]{:S(2)}) copy-start(f32[4,1,128]{2,1,0:T(1,128)} %param.32) | copy-start | bytes 6148
  54.9 37.7 %copy-start.20 = (pred[32,4]{1,0:T(8,128)(4,1)}, pred[32,4]{1,0:T(8,128)(4,1)S(1)}, u32[]{:S(2)}) copy-start(pred[32,4]{1,0:T(8,128)(4,1)S(1)} %copy.167) | copy-start | bytes 388
  55.0 37.9 %copy-start.18 = (pred[32,4]{1,0:T(8,128)(4,1)}, pred[32,4]{1,0:T(8,128)(4,1)S(1)}, u32[]{:S(2)}) copy-start(pred[32,4]{1,0:T(8,128)(4,1)S(1)} %copy.171) | copy-start | bytes 388
  55.1 37.2 %copy-start.22 = (pred[32,4]{1,0:T(8,128)(4,1)}, pred[32,4]{1,0:T(8,128)(4,1)S(1)}, u32[]{:S(2)}) copy-start(pred[32,4]{1,0:T(8,128)(4,1)S(1)} %copy.163) | copy-start | bytes 388
  55.2 36.8 %copy-start.23 = (pred[32,4]{1,0:T(8,128)(4,1)}, pred[32,4]{1,0:T(8,128)(4,1)S(1)}, u32[]{:S(2)}) copy-start(pred[32,4]{1,0:T(8,128)(4,1)S(1)} %copy.158) | copy-start | bytes 388
  55.4 37.4 %copy-start.9 = (s32[32,4]{1,0:T(8,128)}, s32[32,4]{1,0:T(8,128)S(1)}, u32[]{:S(2)}) copy-start(s32[32,4]{1,0:T(8,128)S(1)} %copy.172) | copy-start | bytes 1540
  55.5 37.1 %copy-start.11 = (s32[32,4]{1,0:T(8,128)}, s32[32,4]{1,0:T(8,128)S(1)}, u32[]{:S(2)}) copy-start(s32[32,4]{1,0:T(8,128)S(1)} %copy.168) | copy-start | bytes 1540
  55.6 36.7 %copy-start.13 = (s32[32,4]{1,0:T(8,128)}, s32[32,4]{1,0:T(8,128)S(1)}, u32[]{:S(2)}) copy-start(s32[32,4]{1,0:T(8,128)S(1)} %copy.164) | copy-start | bytes 1540
  55.7 36.3 %copy-start.14 = (s32[32,4]{1,0:T(8,128)}, s32[32,4]{1,0:T(8,128)S(1)}, u32[]{:S(2)}) copy-start(s32[32,4]{1,0:T(8,128)S(1)} %copy.159) | copy-start | bytes 1540
  85.8 5.0 %copy-start.7 = (f32[128]{0:T(128)}, f32[128]{0:T(128)S(1)}, u32[]{:S(2)}) copy-start(f32[128]{0:T(128)S(1)} %rsqrt.18) | copy-start | bytes 1540
  88.0 2.8 %copy-start.3 = (bf16[2048,2,1,64]{0,3,2,1:T(8,128)(2,1)S(1)}, bf16[2048,2,1,64]{0,3,2,1:T(8,128)(2,1)}, u32[]{:S(2)}) copy-start(bf16[2048,2,1,64]{0,3,2,1:T(8,128)(2,1)} %param.25) | copy-start | bytes 1572868
  93.9 10.4 %copy-start.2 = (bf16[2048,2,1,64]{0,3,2,1:T(8,128)(2,1)S(1)}, bf16[2048,2,1,64]{0,3,2,1:T(8,128)(2,1)}, u32[]{:S(2)}) copy-start(bf16[2048,2,1,64]{0,3,2,1:T(8,128)(2,1)} %param.26) | copy-start | bytes 1572868
  94.0 10.2 %copy-start.8 = (f32[128]{0:T(128)S(1)}, f32[128]{0:T(128)}, u32[]{:S(2)}) copy-start(f32[128]{0:T(128)} %copy-done.7) | copy-start | bytes 1540
  95.4 9.2 %copy-start.27 = (f32[2,1]{0,1:T(1,128)S(1)}, f32[2,1]{0,1:T(1,128)}, u32[]{:S(2)}) copy-start(f32[2,1]{0,1:T(1,128)} %param.33) | copy-start | bytes 28
  95.4 9.2 %copy-start.31 = (f32[2]{0:T(128)S(1)}, f32[2]{0:T(128)}, u32[]{:S(2)}) copy-start(f32[2]{0:T(128)} %negate_bitcast_fusion) | copy-start | bytes 28
  104.6 6.4 %copy-start.12 = (s32[32,4]{1,0:T(8,128)S(1)}, s32[32,4]{1,0:T(8,128)}, u32[]{:S(2)}) copy-start(s32[32,4]{1,0:T(8,128)} %copy-done.11) | copy-start | bytes 1540
  104.6 6.4 %copy-start.21 = (pred[32,4]{1,0:T(8,128)(4,1)S(1)}, pred[32,4]{1,0:T(8,128)(4,1)}, u32[]{:S(2)}) copy-start(pred[32,4]{1,0:T(8,128)(4,1)} %copy-done.20) | copy-start | bytes 388
  104.6 6.4 %copy-start.30 = (f32[128]{0:T(128)S(1)}, f32[128]{0:T(128)}, u32[]{:S(2)}) copy-start(f32[128]{0:T(128)} %get-tuple-element.29) | copy-start | bytes 1540
  104.6 6.4 %copy-start.33 = (bf16[32,7,1,128]{3,0,2,1:T(8,128)(2,1)S(1)}, bf16[32,7,1,128]{3,0,2,1:T(8,128)(2,1)}, u32[]{:S(2)}) copy-start(bf16[32,7,1,128]{3,0,2,1:T(8,128)(2,1)} %param.40) | copy-start | bytes 172036
  104.6 6.4 %copy-start.39 = (f32[32,4,128]{2,1,0:T(4,128)S(1)}, f32[32,4,128]{2,1,0:T(4,128)}, u32[]{:S(2)}) copy-start(f32[32,4,128]{2,1,0:T(4,128)} %fusion.57) | copy-start | bytes 196612
  104.6 6.6 %copy-start.10 = (s32[32,4]{1,0:T(8,128)S(1)}, s32[32,4]{1,0:T(8,128)}, u32[]{:S(2)}) copy-start(s32[32,4]{1,0:T(8,128)} %copy-done.9) | copy-start | bytes 1540
  104.6 6.6 %copy-start.19 = (pred[32,4]{1,0:T(8,128)(4,1)S(1)}, pred[32,4]{1,0:T(8,128)(4,1)}, u32[]{:S(2)}) copy-start(pred[32,4]{1,0:T(8,128)(4,1)} %copy-done.18) | copy-start | bytes 388
  104.6 6.6 %copy-start.29 = (f32[128]{0:T(128)S(1)}, f32[128]{0:T(128)}, u32[]{:S(2)}) copy-start(f32[128]{0:T(128)} %get-tuple-element.26) | copy-start | bytes 1540
  104.6 6.6 %copy-start.38 = (f32[32,4,128]{2,1,0:T(4,128)S(1)}, f32[32,4,128]{2,1,0:T(4,128)}, u32[]{:S(2)}) copy-start(f32[32,4,128]{2,1,0:T(4,128)} %fusion.54) | copy-start | bytes 196612
  105.0 6.6 %copy-start.28 = (f32[128]{0:T(128)S(1)}, f32[128]{0:T(128)}, u32[]{:S(2)}) copy-start(f32[128]{0:T(128)} %get-tuple-element.22) | copy-start | bytes 1540
  105.1 6.6 %copy-start.34 = (bf16[32,7,1,128]{3,0,2,1:T(8,128)(2,1)S(1)}, bf16[32,7,1,128]{3,0,2,1:T(8,128)(2,1)}, u32[]{:S(2)}) copy-start(bf16[32,7,1,128]{3,0,2,1:T(8,128)(2,1)} %param.39) | copy-start | bytes 172036
  105.1 6.6 %copy-start.37 = (f32[32,4,128]{2,1,0:T(4,128)S(1)}, f32[32,4,128]{2,1,0:T(4,128)}, u32[]{:S(2)}) copy-start(f32[32,4,128]{2,1,0:T(4,128)} %fusion.55) | copy-start | bytes 196612
  111.3 1.9 %copy-start.5 = (bf16[32,4,2,64]{3,2,1,0:T(2,128)(2,1)S(1)}, bf16[32,4,2,64]{3,2,1,0:T(2,128)(2,1)}, u32[]{:S(2)}) copy-start(bf16[32,4,2,64]{3,2,1,0:T(2,128)(2,1)} %reshape.353) | copy-start | bytes 98308
  111.3 1.9 %copy-start.6 = (f32[32,4,2]{1,2,0:T(2,128)S(1)}, f32[32,4,2]{1,2,0:T(2,128)}, u32[]{:S(2)}) copy-start(f32[32,4,2]{1,2,0:T(2,128)} %copy.185) | copy-start | bytes 3076
  111.3 1.9 %copy-start.15 = (pred[32,4,4]{2,1,0:T(4,128)(4,1)S(1)}, pred[32,4,4]{2,1,0:T(4,128)(4,1)}, u32[]{:S(2)}) copy-start(pred[32,4,4]{2,1,0:T(4,128)(4,1)} %fusion.81) | copy-start | bytes 1540
  112.3 1.2 copy-start.32
  115.2 60.2 %all-to-all-start.1 = ((bf16[32,128,128]{1,2,0:T(8,128)(2,1)}), bf16[32,128,128]{1,2,0:T(8,128)(2,1)S(1)}, u32[]{:S(2)}, u32[]{:S(2)}) async-start(bf16[32,128,128]{1,2,0:T(8,128)(2,1)} %broadcast_in_dim.25), calls=%async_computation.1 | async-start | bytes 2097152 | tf_op jit(solution)/shard_map/all_to_all | solution.py:23
where the time goes:
time: 179 us; the launch traced here: 178 us
  waiting for transfers between devices  70.2 us (39%)
  starting transfers between devices  49.8 us (28%)
  local copies, waits for them, and re-layouts  30.9 us (17%)
  matrix products  20.8 us (12%)
  other arithmetic  5.54 us (3%)
    all_to_all x2, waiting for transfers between devices, from_everyone(): return lax.all_to_all(copies, axis, split_axis=0, concat_axis=0, tiled=True)  70.2 us
    all_to_all x2, starting transfers between devices, from_everyone(): return lax.all_to_all(copies, axis, split_axis=0, concat_axis=0, tiled=True)  49.8 us
    dot_general x11, matrix products, conv_tree(): value = value + jnp.einsum('sjw,swc->sjc', chosen, saved_f)  7.19 us
    dot_general x12, matrix products, conv_tree(): value = jnp.einsum('sji,sic->sjc', onehots[lag], cur_f)  6.92 us
    gather x15, local copies, waits for them, and re-layouts, lineage_tables(): jnp.take_along_axis(predecessor_index, jnp.maximum(current, 0), axis=1)  5.63 us
    convert_element_type x2, local copies, waits for them, and re-layouts, shards(): scaled = (piece_f * gain).astype(jnp.bfloat16).reshape(rows, width)  4.49 us
    reshape x1, local copies, waits for them, and re-layouts, shards(): final_linear_matrix.reshape(kv_count, heads_dev, G, HD, out_cols)  3.89 us
    reshape x1, local copies, waits for them, and re-layouts, shards(): out_flat = jnp.transpose(final_linear_matrix.reshape(kv_count, heads_dev,...  3.87 us
  transfers between devices with their start and end apart: 2, of which 2 were waited for; matrix products, arithmetic and copies ran while one was open for 10% of the time, Pallas kernels for 0%

commit v1 on v0

v1 whole, which is shorter than its diff:
```python
import functools

import jax
import jax.numpy as jnp
from jax import lax
from jax.experimental import pallas as pl
from jax.experimental.pallas import tpu as pltpu
from jax.sharding import PartitionSpec as P

D = 2048
HG = 32
G = 2
HD = 64
N = 128
CONV = 4
WIN = 7
PROP = 4
PREV = 4

INTERPRET = False


def vmem(count):
    return [pl.BlockSpec(memory_space=pltpu.VMEM)] * count


def silu(x):
    return x / (1.0 + jnp.exp(-x))


def pack_kernel(rows_ref, out_ref, wide):
    seqs = rows_ref.shape[0]
    for j in range(PROP):
        wide[j] = rows_ref[:, j, :].astype(jnp.float32)
    packed = jnp.concatenate(
        [
            jnp.concatenate([wide[0], wide[1]], axis=0),
            jnp.concatenate([wide[2], wide[3]], axis=0),
        ],
        axis=1,
    ).astype(jnp.bfloat16)
    for copy in range(out_ref.shape[0]):
        out_ref[copy] = packed


def mixer_kernel(
    pieces_ref,
    gain_ref,
    wx_ref,
    wz_ref,
    wdt_ref,
    wb_ref,
    wc_ref,
    taps_ref,
    heads_ref,
    state_ref,
    mem_x_ref,
    mem_b_ref,
    mem_c_ref,
    table_ref,
    fading_ref,
    out_ref,
    cc_all,
    read_all,
):
    half = pieces_ref.shape[2]
    seqs = half // 2
    rows = 2 * half
    kv_count = pieces_ref.shape[1]
    f32 = jnp.float32
    lane = lax.broadcasted_iota(jnp.int32, (half, 2 * HD), 1)
    left = lane < HD
    scaled = []
    square = jnp.zeros((rows, 2 * HD), f32)
    for k in range(kv_count):
        p0 = pieces_ref[0, k].astype(f32)
        p1 = pieces_ref[1, k].astype(f32)
        top = jnp.where(left, p0, pltpu.roll(p1, HD, 1))
        low = jnp.where(left, pltpu.roll(p0, HD, 1), p1)
        both = jnp.concatenate([top, low], axis=0)
        square = square + both * both
        gain = gain_ref[:, k * 2 * HD : (k + 1) * 2 * HD].astype(f32)
        scaled.append((both * gain).astype(jnp.bfloat16))
    u = jnp.concatenate(scaled, axis=1)
    r_in = lax.rsqrt(jnp.sum(square, axis=1, keepdims=True) / D + 1e-06)

    def times(weight, dims):
        return lax.dot_general(u, weight, dims, preferred_element_type=f32) * r_in

    across = (((1,), (1,)), ((), ()))
    down = (((1,), (0,)), ((), ()))
    x_rows = times(wx_ref[...], across).astype(jnp.bfloat16).astype(f32)
    b_rows = times(wb_ref[...], down).astype(jnp.bfloat16).astype(f32)
    c_rows = times(wc_ref[...], down).astype(jnp.bfloat16).astype(f32)
    z_rows = times(wz_ref[...], across).astype(jnp.bfloat16).astype(f32)
    dt_raw = times(wdt_ref[...], across)

    def wide(column):
        return jnp.broadcast_to(column, (seqs, 2 * HD))

    table = table_ref[...]
    parent = [wide(table[:, j : j + 1]) for j in range(PROP)]
    admitted = wide(table[:, PROP : PROP + 1])
    child = [[parent[j] == i for i in range(j)] for j in range(PROP)]

    def block(array, j):
        return array[j * seqs : (j + 1) * seqs]

    def conv(row_array, mem_ref, first):
        recent = []
        for back in range(CONV - 1):
            offset = CONV - 2 - back
            value = mem_ref[offset].astype(f32)
            for count in range(1, PREV + 1):
                value = jnp.where(admitted == count, mem_ref[offset + count].astype(f32), value)
            recent.append(value)
        history = []
        outs = []
        for j in range(PROP):
            inputs = [block(row_array, j)]
            for back in range(CONV - 1):
                value = recent[back]
                for i in range(j):
                    value = jnp.where(child[j][i], history[i][back], value)
                inputs.append(value)
            history.append(inputs)
            total = None
            for lag in range(CONV):
                tap = taps_ref[first + CONV - 1 - lag : first + CONV - lag, :]
                term = tap * inputs[lag]
                total = term if total is None else total + term
            outs.append(silu(total))
        return outs

    cc = conv(c_rows, mem_c_ref, 2 * CONV)
    for j in range(PROP):
        cc_all[:, j, :] = cc[j]
        cc_all[:, PROP + j, :] = cc[j]
    for s in range(seqs):
        read_all[s] = lax.dot_general(
            cc_all[s].astype(jnp.bfloat16), state_ref[s], across, preferred_element_type=f32
        )
    xc = conv(x_rows, mem_x_ref, 0)
    bc = conv(b_rows, mem_b_ref, CONV)

    offset = heads_ref[0:1, :]
    speed = heads_ref[1:2, :]
    bypass = heads_ref[2:3, :]
    fading = fading_ref[...]
    first_head = left[:seqs]
    level = []
    moved = []
    above = []
    for j in range(PROP):
        raw = block(dt_raw, j) + offset
        step = jnp.maximum(raw, 0.0) + jnp.log1p(jnp.exp(-jnp.abs(raw)))
        extra = jnp.where(
            first_head, wide(fading[:, 2 * j : 2 * j + 1]), wide(fading[:, 2 * j + 1 : 2 * j + 2])
        )
        own = speed * step + extra
        prior = jnp.zeros_like(own)
        for i in range(j):
            prior = jnp.where(child[j][i], level[i], prior)
        level.append(own + prior)
        moved.append(step * xc[j])
        line = []
        for i in range(j):
            reach = child[j][i]
            for p in range(i + 1, j):
                reach = reach | (child[j][p] & above[p][i])
            line.append(reach)
        above.append(line)
    for j in range(PROP):
        y = jnp.exp(level[j]) * read_all[:, j, :] + bypass * xc[j]
        for i in range(j + 1):
            score = jnp.sum(cc[j] * bc[i], axis=1, keepdims=True)
            if i == j:
                y = y + score * moved[i]
            else:
                fall = jnp.exp(jnp.minimum(level[j] - level[i], 0.0))
                y = y + jnp.where(above[j][i], fall * (score * moved[i]), 0.0)
        gated = (y * silu(block(z_rows, j))).astype(jnp.bfloat16)
        for copy in range(out_ref.shape[0]):
            out_ref[copy, j * seqs : (j + 1) * seqs, :] = gated


def last_kernel(tp_ref, own_ref, other_ref, weight_ref, out_ref, spread):
    f32 = jnp.float32
    kv_count, rows = own_ref.shape[0], own_ref.shape[1]
    seqs = rows // PROP
    group = tp_ref[0]
    total = jnp.zeros((rows, weight_ref.shape[1]), f32)
    square = jnp.zeros((rows, 2 * HD), f32)
    for k in range(kv_count):
        lhs = []
        rhs = []
        for ref, t in ((own_ref, group), (other_ref, 1 - group)):
            piece = ref[k]
            wide = piece.astype(f32)
            square = square + wide * wide
            lhs.append(piece)
            for h in range(2):
                start = pl.multiple_of(((2 * k + h) * G + t) * HD, HD)
                rhs.append(weight_ref[pl.ds(start, HD), :])
        total = total + jnp.dot(
            jnp.concatenate(lhs, axis=1), jnp.concatenate(rhs, axis=0), preferred_element_type=f32
        )
    r_out = lax.rsqrt(jnp.sum(square, axis=1, keepdims=True) / (HG * G * HD) + 1e-05)
    mixed = total * r_out
    for j in range(PROP):
        spread[:, j, :] = mixed[j * seqs : (j + 1) * seqs]
    out_ref[...] = spread[...].astype(jnp.bfloat16)


def pack(rows, copies):
    seqs = rows.shape[0]
    return pl.pallas_call(
        pack_kernel,
        out_shape=jax.ShapeDtypeStruct((copies, 2 * seqs, 2 * HD), jnp.bfloat16),
        in_specs=vmem(1),
        out_specs=vmem(1)[0],
        scratch_shapes=[pltpu.VMEM((PROP, seqs, HD), jnp.float32)],
        compiler_params=pltpu.CompilerParams(vmem_limit_bytes=8 << 20),
        interpret=INTERPRET,
        name="pack",
    )(rows)


def mixer(copies, pieces, *rest):
    half = pieces.shape[2]
    return pl.pallas_call(
        mixer_kernel,
        out_shape=jax.ShapeDtypeStruct((copies, 2 * half, 2 * HD), jnp.bfloat16),
        in_specs=vmem(1 + len(rest)),
        out_specs=vmem(1)[0],
        scratch_shapes=[
            pltpu.VMEM((half // 2, 2 * PROP, N), jnp.float32),
            pltpu.VMEM((half // 2, 2 * PROP, 2 * HD), jnp.float32),
        ],
        compiler_params=pltpu.CompilerParams(vmem_limit_bytes=20 << 20),
        cost_estimate=pl.CostEstimate(
            flops=2 * 2 * half * D * 5 * N, bytes_accessed=5 << 20, transcendentals=2 * half * 1000
        ),
        interpret=INTERPRET,
        name="mixer",
    )(pieces, *rest)


def last(group, own, other, weight):
    rows = own.shape[1]
    seqs = rows // PROP
    cols = weight.shape[1]
    return pl.pallas_call(
        last_kernel,
        out_shape=jax.ShapeDtypeStruct((seqs, PROP, cols), jnp.bfloat16),
        in_specs=[pl.BlockSpec(memory_space=pltpu.SMEM)] + vmem(3),
        out_specs=vmem(1)[0],
        scratch_shapes=[pltpu.VMEM((seqs, PROP, cols), jnp.float32)],
        compiler_params=pltpu.CompilerParams(vmem_limit_bytes=20 << 20),
        cost_estimate=pl.CostEstimate(
            flops=2 * rows * HG * G * HD * cols, bytes_accessed=2 << 20, transcendentals=rows
        ),
        interpret=INTERPRET,
        name="last",
    )(group, own, other, weight)


def prepared(
    kv_index,
    tp_index,
    leading_scaling_factor,
    lane_feed_matrix,
    final_valve_matrix,
    increment_matrix,
    entry_basis_matrix,
    readout_basis_matrix,
    lane_feed_kernel,
    entry_basis_kernel,
    readout_basis_kernel,
    increment_offset,
    shrink_speed_exponent,
    lane_bypass_factor,
    hidden_carried_memory,
    lane_filter_memory,
    entry_basis_memory,
    readout_basis_memory,
    predecessor_index,
    admitted_counts,
    surplus_fading,
):
    seqs = predecessor_index.shape[0]
    heads = increment_offset.shape[0]
    wx = jnp.transpose(lane_feed_matrix, (1, 2, 3, 0)).reshape(heads * HD, D)
    wz = jnp.transpose(final_valve_matrix, (1, 2, 3, 0)).reshape(heads * HD, D)
    dt_own = lax.dynamic_slice(
        jnp.transpose(increment_matrix, (1, 2, 0)), (kv_index * heads, tp_index, 0), (heads, 1, D)
    )
    wdt = jnp.broadcast_to(dt_own, (heads, HD, D)).reshape(heads * HD, D)
    wb = entry_basis_matrix.reshape(D, N)
    wc = readout_basis_matrix.reshape(D, N)
    taps = jnp.concatenate(
        [
            lane_feed_kernel.reshape(CONV, heads * HD),
            entry_basis_kernel.reshape(CONV, N),
            readout_basis_kernel.reshape(CONV, N),
        ],
        axis=0,
    )

    def per_lane(values):
        return jnp.broadcast_to(values, (heads, HD)).reshape(1, heads * HD)

    head_rows = jnp.concatenate(
        [
            per_lane(increment_offset),
            per_lane(-jnp.exp(shrink_speed_exponent)),
            per_lane(lane_bypass_factor),
        ],
        axis=0,
    )
    state = hidden_carried_memory.reshape(seqs, heads * HD, N).astype(jnp.bfloat16)
    mem_x = jnp.transpose(lane_filter_memory, (1, 0, 2, 3, 4)).reshape(WIN, seqs, heads * HD)
    mem_b = jnp.transpose(entry_basis_memory, (1, 0, 2, 3)).reshape(WIN, seqs, N)
    mem_c = jnp.transpose(readout_basis_memory, (1, 0, 2, 3)).reshape(WIN, seqs, N)
    table = jnp.concatenate([predecessor_index, admitted_counts[:, None]], axis=1)
    fading = surplus_fading.reshape(seqs, PROP * heads)
    return (
        leading_scaling_factor.reshape(1, D),
        wx,
        wz,
        wdt,
        wb,
        wc,
        taps,
        head_rows,
        state,
        mem_x,
        mem_b,
        mem_c,
        table,
        fading,
    )


def shards(candidate_vectors, leading_scaling_factor, lane_feed_matrix, final_valve_matrix,
           increment_matrix, entry_basis_matrix, readout_basis_matrix, lane_feed_kernel,
           entry_basis_kernel, readout_basis_kernel, increment_offset, shrink_speed_exponent,
           lane_bypass_factor, final_linear_matrix, *memories):
    kv_count = lax.axis_size("kv")
    copies = pack(candidate_vectors, kv_count)
    along = lax.all_to_all(copies, "kv", split_axis=0, concat_axis=0, tiled=True)
    pieces = lax.all_gather(along, "tp")
    rest = prepared(
        lax.axis_index("kv"), lax.axis_index("tp"), leading_scaling_factor, lane_feed_matrix,
        final_valve_matrix, increment_matrix, entry_basis_matrix, readout_basis_matrix,
        lane_feed_kernel, entry_basis_kernel, readout_basis_kernel, increment_offset,
        shrink_speed_exponent, lane_bypass_factor, *memories,
    )
    gated = mixer(1, pieces, *rest)
    along = lax.all_gather(gated[0], "kv")
    swapped = lax.ppermute(along, "tp", [(0, 1), (1, 0)])
    weight = final_linear_matrix.reshape(HG * G * HD, -1)
    return last(lax.axis_index("tp").reshape(1), along, swapped, weight)


def solution(mesh):
    placed = (
        P(("grp", "dp"), None, ("kv", "tp")),
        P(),
        P(None, "kv", "tp", None),
        P(None, "kv", "tp", None),
        P(),
        P(None, "tp", None),
        P(None, "tp", None),
        P(None, "kv", "tp", None),
        P(None, "tp", None),
        P(None, "tp", None),
        P("kv", "tp"),
        P("kv", "tp"),
        P("kv", "tp"),
        P(None, None, None, ("kv", "tp")),
        P(("grp", "dp"), "kv", "tp", None, None),
        P(("grp", "dp"), None, "kv", "tp", None),
        P(("grp", "dp"), None, "tp", None),
        P(("grp", "dp"), None, "tp", None),
        P(("grp", "dp"), None),
        P(("grp", "dp")),
        P(("grp", "dp"), None, "kv", "tp"),
    )
    return jax.shard_map(
        shards,
        mesh=mesh,
        in_specs=placed,
        out_specs=P(("grp", "dp"), None, ("kv", "tp")),
        check_vma=False,
    )
```

time: 179 us -> 111 us (0.62)
  waiting for transfers between devices: 70.2 us -> 1.52 us
  blocking collectives: 0 us -> 31.8 us
  matrix products: 20.8 us -> 0 us
  local copies, waits for them, and re-layouts: 30.9 us -> 12.8 us
  Pallas kernels: 0 us -> 3.62 us
  starting transfers between devices: 49.8 us -> 53.4 us
    all_to_all x2 -> x1, waiting for transfers between devices: 70.2 us -> 0.01 us  [shards(): lax.all_to_all(copies, 'kv', split_axis=0, concat_axis=0, tiled=True)]
    all_gather x0 -> x2, blocking collectives: none -> 31.8 us  [the longest x1 25.3 us: shards(): along = lax.all_gather(gated[0], 'kv')]
    dot_general x33 -> x0, matrix products: 20.8 us -> none  [the longest x11 7.19 us: conv_tree(): value = value + jnp.einsum('sjw,swc->sjc', chosen, saved_f)]
    ppermute x0 -> x1, starting transfers between devices: none -> 9.22 us  [shards(): swapped = lax.ppermute(along, 'tp', [(0, 1), (1, 0)])]
    gather x15 -> x0, local copies, waits for them, and re-layouts: 5.63 us -> none  [lineage_tables(): jnp.take_along_axis(predecessor_index, jnp.maximum(current, 0), axis=1)]
    all_to_all x2 -> x1, starting transfers between devices: 49.8 us -> 44.2 us  [shards(): lax.all_to_all(copies, 'kv', split_axis=0, concat_axis=0, tiled=True)]
    convert_element_type x5 -> x0, local copies, waits for them, and re-layouts: 5.39 us -> none  [the longest x2 4.49 us: shards(): scaled = (piece_f * gain).astype(jnp.bfloat16).reshape(rows, width)]
    pallas_call x0 -> x3, Pallas kernels: none -> 3.62 us  [the longest x1 1.72 us: mixer(): pl.pallas_call(mixer_kernel, out_shape=jax.ShapeDtypeStruct((copies, 2 *...]
  transfers between devices with their start and end apart: 2 -> 2, of which waited for: 2 -> 1; matrix products, arithmetic and copies ran while one was open for 10% -> 14% of each run, Pallas kernels for 0% -> 0%
where the time goes in v1:
time: 111 us; the launch traced here: 110 us
  starting transfers between devices  53.4 us (48%)
  blocking collectives  31.8 us (29%)
  local copies, waits for them, and re-layouts  12.8 us (12%)
  other arithmetic  6.55 us (6%)
  Pallas kernels  3.62 us (3%)
  waiting for transfers between devices  1.52 us (1%)
    all_to_all x1, starting transfers between devices, shards(): lax.all_to_all(copies, 'kv', split_axis=0, concat_axis=0, tiled=True)  44.2 us
    all_gather x1, blocking collectives, shards(): along = lax.all_gather(gated[0], 'kv')  25.3 us
    ppermute x1, starting transfers between devices, shards(): swapped = lax.ppermute(along, 'tp', [(0, 1), (1, 0)])  9.22 us
    all_gather x1, blocking collectives, shards(): pieces = lax.all_gather(along, 'tp')  6.43 us
    unnamed x34, local copies, waits for them, and re-layouts  4.84 us
  transfers between devices with their start and end apart: 2, of which 1 were waited for; matrix products, arithmetic and copies ran while one was open for 14% of the time, Pallas kernels for 0%

profile of v1, /device:TPU:65, one launch (start us, length us, event | category | flops | bytes accessed | tf_op | source)
XLA Modules:
  0.0 109.9 jit_solution(18130770449066469184)
XLA Ops:
  0.0 0.0 copy-start
  0.0 0.0 copy-start.10
  0.0 0.8 copy-done.10
  0.8 0.8 pack.1
  1.6 44.2 %all-to-all-start = ((bf16[16,64,128]{2,1,0:T(8,128)(2,1)}), bf16[16,64,128]{2,1,0:T(8,128)(2,1)}, u32[]{:S(2)}, u32[]{:S(2)}) async-start(bf16[16,64,128]{2,1,0:T(8,128)(2,1)} %pack.1), calls=%async_computation | async-start | bytes 524288 | tf_op jit(solution)/shard_map/all_to_all | solution.py:351
  45.9 0.7 negate_bitcast_fusion
  46.5 0.1 broadcast_in_dim.36
  46.6 0.7 reshape.67
  47.2 0.7 broadcast_in_dim.34
  48.0 0.6 reshape.66
  48.6 0.7 broadcast_in_dim.38
  49.3 0.7 reshape.68
  49.9 0.5 broadcast.3
  50.4 1.4 %reduce.3 = f32[4,2,64]{2,1,0:T(2,128)S(1)} reduce(f32[4,2,1,64]{3,2,1,0:T(1,128)} %param.28, f32[]{:T(128)} %broadcast.3), dimensions={2}, to_apply=%param.28.reduce_sub_computation.3 | reduce | bytes 4100 | tf_op args[7]
  51.8 0.6 reshape.63
  52.4 1.3 %reshape.57.gain_ref = bf16[1,2048]{1,0:T(2,128)(2,1)} reshape(bf16[2048]{0:T(1024)(128)(2,1)} %param.22) | data formatting | bytes 8192 | tf_op jit(solution)/shard_map/reshape | solution.py:328
  53.7 0.7 pad_add_fusion
  54.4 0.1 copy.37.table_ref
  54.5 0.0 copy-done
  54.6 0.6 copy.42
  55.2 0.8 copy.38.fading_ref
  55.9 1.0 reshape.75
  57.0 0.0 copy-start.13
  57.0 0.0 copy-start.14
  57.0 0.0 copy-start.15
  57.0 0.0 copy-start.12
  57.0 0.0 copy-start.2
  57.0 0.0 copy-start.3
  57.0 0.0 copy-start.4
  57.0 0.0 copy-start.5
  57.1 0.0 copy-start.6
  57.1 1.9 %convert_element_type.5 = bf16[32,2,1,64,128]{4,3,2,1,0:T(8,128)(2,1)S(1)} convert(f32[32,2,1,64,128]{4,3,2,1,0:T(8,128)} %param.35) | non-fusion elementwise | flops 524288 | bytes 3145728 | tf_op jit(solution)/shard_map/convert_element_type | solution.py:321
  59.0 0.0 copy-done.13
  59.0 0.0 copy-done.14
  59.0 0.0 copy-done.15
  59.1 0.6 pad_maximum_fusion.1.heads_ref
  59.6 0.0 copy-done.12
  59.6 1.3 %pad_maximum_fusion.taps_ref = f32[12,128]{1,0:T(8,128)} fusion(f32[4,128]{1,0:T(4,128)} %bitcast.52, f32[4,128]{1,0:T(4,128)} %bitcast.53, f32[4,128]{1,0:T(4,128)S(1)} %copy-done.12), kind=kLoop, calls=%fused_computation.1 | loop fusion | flops 3072 | bytes 12288 | tf_op jit(solution)/shard_map/concatenate | solution.py:301
  60.9 0.0 all-to-all-done
  60.9 6.4 %all-gather = bf16[32,64,128]{2,1,0:T(8,128)(2,1)S(1)} all-gather(bf16[16,64,128]{2,1,0:T(8,128)(2,1)} %all-to-all-done), channel_id=2, replica_groups=mesh['grp'=2,'dp'=8,'kv'=16,'tp'=2] {'tp'}, dimensions={0}, use_global_device_ids=true | all-gather | bytes 786432 | tf_op jit(solution)/shard_map/all_gather | solution.py:352
  67.4 0.7 broadcast_in_dim.32
  68.1 0.0 copy-done.2
  68.1 0.0 copy-done.3
  68.1 0.0 copy-done.4
  68.1 0.0 copy-done.5
  68.2 0.0 copy-done.6
  68.2 0.0 copy-start.7
  68.2 0.8 copy-done.7
  69.0 0.0 copy-start.8
  69.0 0.7 copy-done.8
  69.7 0.0 copy-start.9
  69.7 0.7 copy-done.9
  70.4 0.0 copy-start.11
  70.4 0.7 copy-done.11
  71.1 0.0 copy-start.1
  71.1 1.7 %mixer.1 = bf16[1,128,128]{2,1,0:T(8,128)(2,1)S(1)} custom-call(bf16[2,16,64,128]{3,2,1,0:T(8,128)(2,1)S(1)} %bitcast.40, bf16[1,2048]{1,0:T(2,128)(2,1)S(1)} %copy-done.9, bf16[128,2048]{1,0:T(8,128)(2,1)S(1)} %bitcast.43, bf16[128,2048]{1,0:T(8,128)(2,1)S(1)} %bitcast.44, bf16[128,2048]{1,0:T(8,128)(2,1)S(1)} %bitcast.41, bf16[2048,128]{1,0:T(8,128)(2,1)S(1)} %bitcast.45, ...), custom_call_target="tpu_custom_call" | custom-call | flops 335544320 | bytes 5242880 | tf_op jit(solution)/shard_map/mixer/pallas_call | solution.py:231
  72.8 25.3 %all_gather.11.own_ref = bf16[16,128,128]{2,1,0:T(8,128)(2,1)S(1)} all-gather(bf16[1,128,128]{2,1,0:T(8,128)(2,1)S(1)} %mixer.1), channel_id=1, replica_groups=mesh['grp'=2,'dp'=8,'kv'=16,'tp'=2] {'kv'}, dimensions={0}, use_global_device_ids=true | all-gather | bytes 557056 | tf_op jit(solution)/shard_map/all_gather | solution.py:360
  98.1 9.2 %collective-permute-start = (bf16[16,128,128]{2,1,0:T(8,128)(2,1)S(1)}, bf16[16,128,128]{2,1,0:T(8,128)(2,1)S(1)}, u32[]{:S(2)}, u32[]{:S(2)}) collective-permute-start(bf16[16,128,128]{2,1,0:T(8,128)(2,1)S(1)} %all_gather.11.own_ref), channel_id=1, source_target_pairs={{0,1},{1,0},{2,3},{3,2},{4,5},{5,4},{6,7},{7,6},{8,9},{9,8},{10,11... | collective-permute-start | bytes 1572872 | tf_op jit(solution)/shard_map/ppermute | solution.py:361
  107.3 1.5 %collective-permute-done.other_ref = bf16[16,128,128]{2,1,0:T(8,128)(2,1)S(1)} collective-permute-done((bf16[16,128,128]{2,1,0:T(8,128)(2,1)S(1)}, bf16[16,128,128]{2,1,0:T(8,128)(2,1)S(1)}, u32[]{:S(2)}, u32[]{:S(2)}) %collective-permute-start) | collective-permute-done | bytes 524320 | tf_op jit(solution)/shard_map/ppermute | solution.py:361
  108.9 0.0 copy-done.1
  108.9 1.1 last.1
  (2 shorter events, 0.0 us)
Async XLA Ops:
  0.0 54.5 %copy-start = (bf16[2048,32,2]{0,2,1:T(2,128)(2,1)S(1)}, bf16[2048,32,2]{0,2,1:T(2,128)(2,1)}, u32[]{:S(2)}) copy-start(bf16[2048,32,2]{0,2,1:T(2,128)(2,1)} %param.25) | copy-start | bytes 786436
  0.0 0.8 copy-start.10
  1.6 59.3 %all-to-all-start = ((bf16[16,64,128]{2,1,0:T(8,128)(2,1)}), bf16[16,64,128]{2,1,0:T(8,128)(2,1)}, u32[]{:S(2)}, u32[]{:S(2)}) async-start(bf16[16,64,128]{2,1,0:T(8,128)(2,1)} %pack.1), calls=%async_computation | async-start | bytes 524288 | tf_op jit(solution)/shard_map/all_to_all | solution.py:351
  57.0 2.1 %copy-start.13 = (f32[1,128]{1,0:T(1,128)S(1)}, f32[1,128]{1,0:T(1,128)}, u32[]{:S(2)}) copy-start(f32[1,128]{1,0:T(1,128)} %reshape.67) | copy-start | bytes 1540
  57.0 2.1 %copy-start.14 = (f32[1,128]{1,0:T(1,128)S(1)}, f32[1,128]{1,0:T(1,128)}, u32[]{:S(2)}) copy-start(f32[1,128]{1,0:T(1,128)} %reshape.66) | copy-start | bytes 1540
  57.0 2.1 %copy-start.15 = (f32[1,128]{1,0:T(1,128)S(1)}, f32[1,128]{1,0:T(1,128)}, u32[]{:S(2)}) copy-start(f32[1,128]{1,0:T(1,128)} %reshape.68) | copy-start | bytes 1540
  57.0 2.7 %copy-start.12 = (f32[4,128]{1,0:T(4,128)S(1)}, f32[4,128]{1,0:T(4,128)}, u32[]{:S(2)}) copy-start(f32[4,128]{1,0:T(4,128)} %reshape.63) | copy-start | bytes 6148
  57.0 11.1 %copy-start.2 = (bf16[2048,2,1,64]{0,3,2,1:T(8,128)(2,1)S(1)}, bf16[2048,2,1,64]{0,3,2,1:T(8,128)(2,1)}, u32[]{:S(2)}) copy-start(bf16[2048,2,1,64]{0,3,2,1:T(8,128)(2,1)} %param.23) | copy-start | bytes 1572868
  57.0 11.1 %copy-start.3 = (bf16[2048,2,1,64]{0,3,2,1:T(8,128)(2,1)S(1)}, bf16[2048,2,1,64]{0,3,2,1:T(8,128)(2,1)}, u32[]{:S(2)}) copy-start(bf16[2048,2,1,64]{0,3,2,1:T(8,128)(2,1)} %param.24) | copy-start | bytes 1572868
  57.0 11.1 %copy-start.4 = (bf16[2048,1,128]{2,0,1:T(8,128)(2,1)S(1)}, bf16[2048,1,128]{2,0,1:T(8,128)(2,1)}, u32[]{:S(2)}) copy-start(bf16[2048,1,128]{2,0,1:T(8,128)(2,1)} %param.26) | copy-start | bytes 1572868
  57.0 11.1 %copy-start.5 = (bf16[2048,1,128]{2,0,1:T(8,128)(2,1)S(1)}, bf16[2048,1,128]{2,0,1:T(8,128)(2,1)}, u32[]{:S(2)}) copy-start(bf16[2048,1,128]{2,0,1:T(8,128)(2,1)} %param.27) | copy-start | bytes 1572868
  57.1 11.1 %copy-start.6 = (bf16[32,7,1,128]{3,0,2,1:T(8,128)(2,1)S(1)}, bf16[32,7,1,128]{3,0,2,1:T(8,128)(2,1)}, u32[]{:S(2)}) copy-start(bf16[32,7,1,128]{3,0,2,1:T(8,128)(2,1)} %param.37) | copy-start | bytes 172036
  68.2 0.8 copy-start.7
  69.0 0.7 copy-start.8
  69.7 0.7 copy-start.9
  70.4 0.7 copy-start.11
  71.1 37.8 %copy-start.1 = (bf16[32,2,64,64]{3,2,1,0:T(8,128)(2,1)S(1)}, bf16[32,2,64,64]{3,2,1,0:T(8,128)(2,1)}, u32[]{:S(2)}) copy-start(bf16[32,2,64,64]{3,2,1,0:T(8,128)(2,1)} %param.34) | copy-start | bytes 1572868
  98.1 10.7 %collective-permute-start = (bf16[16,128,128]{2,1,0:T(8,128)(2,1)S(1)}, bf16[16,128,128]{2,1,0:T(8,128)(2,1)S(1)}, u32[]{:S(2)}, u32[]{:S(2)}) collective-permute-start(bf16[16,128,128]{2,1,0:T(8,128)(2,1)S(1)} %all_gather.11.own_ref), channel_id=1, source_target_pairs={{0,1},{1,0},{2,3},{3,2},{4,5},{5,4},{6,7},{7,6},{8,9},{9,8},{10,11... | collective-permute-start | bytes 1572872 | tf_op jit(solution)/shard_map/ppermute | solution.py:361

commit v2 on v1

v2 whole, which is shorter than its diff:
```python
import functools

import jax
import jax.numpy as jnp
from jax import lax
from jax.experimental import pallas as pl
from jax.experimental.pallas import tpu as pltpu
from jax.sharding import Mesh
from jax.sharding import PartitionSpec as P

D = 2048
HG = 32
G = 2
HD = 64
N = 128
CONV = 4
WIN = 7
PROP = 4
PREV = 4

KV = ("far", "near")

INTERPRET = False


def vmem(count):
    return [pl.BlockSpec(memory_space=pltpu.VMEM)] * count


def in_vmem(x):
    return x if INTERPRET else pltpu.with_memory_space_constraint(x, pltpu.VMEM)


def in_hbm(x):
    return x if INTERPRET else pltpu.with_memory_space_constraint(x, pltpu.HBM)


def pack_kernel(rows_ref, out_ref, wide):
    seqs = rows_ref.shape[0]
    for j in range(PROP):
        wide[j] = rows_ref[:, j, :].astype(jnp.float32)
    packed = jnp.concatenate(
        [
            jnp.concatenate([wide[0], wide[1]], axis=0),
            jnp.concatenate([wide[2], wide[3]], axis=0),
        ],
        axis=1,
    ).astype(jnp.bfloat16)
    for copy in range(out_ref.shape[0]):
        out_ref[copy] = packed


def places(seqs):
    at, row = {}, 0
    sizes = (("gain", D // N), ("taps", 16), ("heads", 8), ("fading", PROP * seqs), ("end", 0))
    for name, size in sizes:
        at[name] = row
        row += size
    return at


def prep_kernel(*refs):
    count = 13
    sources, held, sems = refs[:count], refs[count + 3 : -1], refs[-1]
    wide_out, narrow_out, recent_out = refs[count : count + 3]
    copies = [pltpu.make_async_copy(sources[k], held[k], sems.at[k]) for k in range(count)]
    for copy in copies:
        copy.start()
    (
        gain_ref,
        dt_ref,
        mem_x_ref,
        mem_b_ref,
        mem_c_ref,
        taps_x_ref,
        taps_b_ref,
        taps_c_ref,
        heads_ref,
        parents_ref,
        admitted_ref,
        fading_ref,
        state_ref,
    ) = held
    f32 = jnp.float32
    seqs = state_ref.shape[0]
    at = places(seqs)
    for copy in copies[:-1]:
        copy.wait()
    def put(name, index, value):
        start = at[name] + index * value.shape[0]
        wide_out[start : start + value.shape[0], :] = value

    for k in range(D // N):
        put("gain", k, gain_ref[:, k * N : (k + 1) * N].astype(f32))
        pair = [
            jnp.broadcast_to(dt_ref[h : h + 1, k * N : (k + 1) * N].astype(f32), (8, N))
            for h in range(2)
        ]
        row = (k % 8) * 16
        narrow_out[seqs + k // 8, row : row + 16, :] = jnp.concatenate(pair, axis=0).astype(
            jnp.bfloat16
        )
    for t in range(CONV):
        put("taps", t, jnp.concatenate([taps_x_ref[t, h] for h in range(2)], axis=1))
        put("taps", CONV + t, taps_b_ref[t])
        put("taps", 2 * CONV + t, taps_c_ref[t])
    one = lax.broadcasted_iota(jnp.int32, (1, 2 * HD), 1) < HD
    heads = heads_ref[...]
    for place in range(3):
        row = jnp.where(one, heads[place : place + 1, 0:1], heads[place : place + 1, 1:2])
        put("heads", place, -jnp.exp(row) if place == 1 else row)

    def turned(lines):
        total = sum(line.shape[0] for line in lines)
        if total < 8:
            lines = lines + [jnp.zeros((8 - total, seqs), f32)]
        lines = jnp.concatenate(lines, axis=0)
        lines = jnp.concatenate([lines, jnp.zeros((8, N - seqs), f32)], axis=1)
        return jnp.transpose(lines)[:seqs]

    def wide(column):
        return jnp.broadcast_to(column, (seqs, 2 * HD))

    table = turned([parents_ref[...].astype(f32), admitted_ref[...].astype(f32)])
    admitted = wide(table[:, PROP : PROP + 1])
    for j in range(PROP):
        start = 3 * (CONV - 1) + j
        recent_out[start * seqs : (start + 1) * seqs, :] = wide(table[:, j : j + 1]).astype(jnp.bfloat16)
    for which, mem_ref in enumerate((mem_x_ref, mem_b_ref, mem_c_ref)):
        for back in range(CONV - 1):
            offset = CONV - 2 - back
            value = mem_ref[offset].astype(f32)
            for step in range(1, PREV + 1):
                value = jnp.where(admitted == step, mem_ref[offset + step].astype(f32), value)
            start = which * (CONV - 1) + back
            recent_out[start * seqs : (start + 1) * seqs, :] = value.astype(jnp.bfloat16)
    fading = turned([fading_ref[j, h] for j in range(PROP) for h in range(2)])
    first_head = lax.broadcasted_iota(jnp.int32, (seqs, 2 * HD), 1) < HD
    for j in range(PROP):
        pair = [wide(fading[:, 2 * j + h : 2 * j + h + 1]) for h in range(2)]
        put("fading", j, jnp.where(first_head, *pair))
    copies[-1].wait()
    narrow_out[:seqs] = state_ref[...].astype(jnp.bfloat16)


def mixer_kernel(
    pieces_ref,
    wx_ref,
    wz_ref,
    wb_ref,
    wc_ref,
    wide_ref,
    narrow_ref,
    recent_ref,
    out_ref,
    cc_all,
    read_all,
    wz_held,
    wz_sem,
):
    half = pieces_ref.shape[2]
    seqs = half // 2
    rows = 2 * half
    kv_count = pieces_ref.shape[1]
    f32 = jnp.float32
    wz_copy = pltpu.make_async_copy(wz_ref, wz_held, wz_sem)
    wz_copy.start()
    left = lax.broadcasted_iota(jnp.int32, (half, 2 * HD), 1) < HD
    at = places(seqs)

    def table(name, index, size):
        return wide_ref[at[name] + index * size : at[name] + (index + 1) * size, :]

    scaled = []
    square = jnp.zeros((rows, 2 * HD), f32)
    for k in range(kv_count):
        p0 = pieces_ref[0, k].astype(f32)
        p1 = pieces_ref[1, k].astype(f32)
        top = jnp.where(left, p0, pltpu.roll(p1, HD, 1))
        low = jnp.where(left, pltpu.roll(p0, HD, 1), p1)
        both = jnp.concatenate([top, low], axis=0)
        square = square + both * both
        gain = table("gain", k, 1)
        scaled.append((both * gain).astype(jnp.bfloat16))
    u = jnp.concatenate(scaled, axis=1)
    r_in = lax.rsqrt(jnp.sum(square, axis=1, keepdims=True) / D + 1e-06)

    def times(weight, dims):
        return lax.dot_general(u, weight, dims, preferred_element_type=f32) * r_in

    across = (((1,), (1,)), ((), ()))
    down = (((1,), (0,)), ((), ()))
    c_rows = times(wc_ref[...], down).astype(jnp.bfloat16).astype(f32)
    b_rows = times(wb_ref[...], down).astype(jnp.bfloat16).astype(f32)
    x_rows = times(wx_ref[...], across).astype(jnp.bfloat16).astype(f32)
    chunks = [narrow_ref[seqs + k // 8, (k % 8) * 16 : (k % 8) * 16 + 16, :] for k in range(D // N)]
    dt_cols = times(jnp.concatenate(chunks, axis=1), across)
    dt_raw = jnp.where(
        lax.broadcasted_iota(jnp.int32, (rows, 2 * HD), 1) < HD,
        *(jnp.broadcast_to(dt_cols[:, c : c + 1], (rows, 2 * HD)) for c in (0, 8)),
    )

    def recent(index):
        return recent_ref[index * seqs : (index + 1) * seqs, :].astype(f32)

    parent = [recent(3 * (CONV - 1) + j) for j in range(PROP)]
    child = [[parent[j] == i for i in range(j)] for j in range(PROP)]

    def block(array, j):
        return array[j * seqs : (j + 1) * seqs]

    def conv(row_array, which):
        history = []
        outs = []
        roots = [recent(which * (CONV - 1) + back) for back in range(CONV - 1)]
        for j in range(PROP):
            inputs = [block(row_array, j)]
            for back in range(CONV - 1):
                value = roots[back]
                for i in range(j):
                    value = jnp.where(child[j][i], history[i][back], value)
                inputs.append(value)
            history.append(inputs)
            total = None
            for lag in range(CONV):
                term = table("taps", which * CONV + CONV - 1 - lag, 1) * inputs[lag]
                total = term if total is None else total + term
            outs.append(jax.nn.silu(total))
        return outs

    cc = conv(c_rows, 2)
    for j in range(PROP):
        cc_all[:, j, :] = cc[j]
        cc_all[:, PROP + j, :] = cc[j]
    for s in range(seqs):
        read_all[s] = lax.dot_general(
            cc_all[s].astype(jnp.bfloat16), narrow_ref[s], across, preferred_element_type=f32
        )
    xc = conv(x_rows, 0)
    bc = conv(b_rows, 1)

    offset, speed, bypass = (table("heads", place, 1) for place in range(3))
    level = []
    moved = []
    above = []
    for j in range(PROP):
        raw = block(dt_raw, j) + offset
        step = jnp.maximum(raw, 0.0) + jnp.log1p(jnp.exp(-jnp.abs(raw)))
        own = speed * step + table("fading", j, seqs)
        prior = jnp.zeros_like(own)
        for i in range(j):
            prior = jnp.where(child[j][i], level[i], prior)
        level.append(own + prior)
        moved.append(step * xc[j])
        line = []
        for i in range(j):
            reach = child[j][i]
            for p in range(i + 1, j):
                reach = reach | (child[j][p] & above[p][i])
            line.append(reach)
        above.append(line)
    wz_copy.wait()
    z_rows = times(wz_held[...], across).astype(jnp.bfloat16).astype(f32)
    for j in range(PROP):
        y = jnp.exp(level[j]) * read_all[:, j, :] + bypass * xc[j]
        for i in range(j + 1):
            score = jnp.sum(cc[j] * bc[i], axis=1, keepdims=True)
            if i == j:
                y = y + score * moved[i]
            else:
                fall = jnp.exp(jnp.minimum(level[j] - level[i], 0.0))
                y = y + jnp.where(above[j][i], fall * (score * moved[i]), 0.0)
        gated = (y * jax.nn.silu(block(z_rows, j))).astype(jnp.bfloat16)
        out_ref[j * seqs : (j + 1) * seqs, :] = gated


def last_kernel(tp_ref, own_ref, other_ref, weight_ref, out_ref, spread):
    f32 = jnp.float32
    near, far, rows = own_ref.shape[:3]
    seqs = rows // PROP
    group = tp_ref[0]
    total = jnp.zeros((rows, weight_ref.shape[1]), f32)
    square = jnp.zeros((rows, 2 * HD), f32)
    for k in range(near * far):
        lhs = []
        rhs = []
        for ref, t in ((own_ref, group), (other_ref, 1 - group)):
            piece = ref[k % near, k // near]
            wide = piece.astype(f32)
            square = square + wide * wide
            lhs.append(piece)
            for h in range(2):
                start = pl.multiple_of(((2 * k + h) * G + t) * HD, HD)
                rhs.append(weight_ref[pl.ds(start, HD), :])
        total = total + jnp.dot(
            jnp.concatenate(lhs, axis=1), jnp.concatenate(rhs, axis=0), preferred_element_type=f32
        )
    r_out = lax.rsqrt(jnp.sum(square, axis=1, keepdims=True) / (HG * G * HD) + 1e-05)
    mixed = total * r_out
    for j in range(PROP):
        spread[:, j, :] = mixed[j * seqs : (j + 1) * seqs]
    out_ref[...] = spread[...].astype(jnp.bfloat16)


def pack(rows, copies):
    seqs = rows.shape[0]
    return pl.pallas_call(
        pack_kernel,
        out_shape=jax.ShapeDtypeStruct((copies, 2 * seqs, 2 * HD), jnp.bfloat16),
        in_specs=vmem(1),
        out_specs=vmem(1)[0],
        scratch_shapes=[pltpu.VMEM((PROP, seqs, HD), jnp.float32)],
        compiler_params=pltpu.CompilerParams(vmem_limit_bytes=8 << 20),
        interpret=INTERPRET,
        name="pack",
    )(rows)


def prep(*inputs):
    state = inputs[-1]
    seqs = state.shape[0]
    return pl.pallas_call(
        prep_kernel,
        out_shape=[
            pltpu.VMEM((places(seqs)["end"], N), jnp.float32),
            pltpu.VMEM((seqs + D // N // 8, N, N), jnp.bfloat16),
            pltpu.VMEM(((3 * (CONV - 1) + PROP) * seqs, N), jnp.bfloat16),
        ],
        in_specs=[pl.BlockSpec(memory_space=pltpu.HBM)] * len(inputs),
        out_specs=vmem(3),
        scratch_shapes=[pltpu.VMEM(x.shape, x.dtype) for x in inputs]
        + [pltpu.SemaphoreType.DMA((len(inputs),))],
        compiler_params=pltpu.CompilerParams(vmem_limit_bytes=16 << 20),
        cost_estimate=pl.CostEstimate(flops=1 << 24, bytes_accessed=4 << 20, transcendentals=0),
        interpret=INTERPRET,
        name="prep",
    )(*(in_hbm(x) for x in inputs))


def mixer(pieces, *rest):
    half = pieces.shape[2]
    return pl.pallas_call(
        mixer_kernel,
        out_shape=jax.ShapeDtypeStruct((2 * half, 2 * HD), jnp.bfloat16),
        in_specs=vmem(2) + [pl.BlockSpec(memory_space=pltpu.HBM)] + vmem(len(rest) - 2),
        out_specs=vmem(1)[0],
        scratch_shapes=[
            pltpu.VMEM((half // 2, 2 * PROP, N), jnp.float32),
            pltpu.VMEM((half // 2, 2 * PROP, 2 * HD), jnp.float32),
            pltpu.VMEM((2 * HD, D), jnp.bfloat16),
            pltpu.SemaphoreType.DMA,
        ],
        compiler_params=pltpu.CompilerParams(vmem_limit_bytes=20 << 20),
        cost_estimate=pl.CostEstimate(
            flops=2 * 2 * half * D * 5 * N, bytes_accessed=5 << 20, transcendentals=2 * half * 1000
        ),
        interpret=INTERPRET,
        name="mixer",
    )(pieces, *rest)


def last(group, own, other, weight):
    rows = own.shape[2]
    seqs = rows // PROP
    cols = weight.shape[1]
    return pl.pallas_call(
        last_kernel,
        out_shape=jax.ShapeDtypeStruct((seqs, PROP, cols), jnp.bfloat16),
        in_specs=[pl.BlockSpec(memory_space=pltpu.SMEM)] + vmem(3),
        out_specs=vmem(1)[0],
        scratch_shapes=[pltpu.VMEM((seqs, PROP, cols), jnp.float32)],
        compiler_params=pltpu.CompilerParams(vmem_limit_bytes=20 << 20),
        cost_estimate=pl.CostEstimate(
            flops=2 * rows * HG * G * HD * cols, bytes_accessed=2 << 20, transcendentals=rows
        ),
        interpret=INTERPRET,
        name="last",
    )(group, own, other, weight)


def prepared(
    kv_index,
    tp_index,
    leading_scaling_factor,
    lane_feed_matrix,
    final_valve_matrix,
    increment_matrix,
    entry_basis_matrix,
    readout_basis_matrix,
    lane_feed_kernel,
    entry_basis_kernel,
    readout_basis_kernel,
    increment_offset,
    shrink_speed_exponent,
    lane_bypass_factor,
    hidden_carried_memory,
    lane_filter_memory,
    entry_basis_memory,
    readout_basis_memory,
    predecessor_index,
    admitted_counts,
    surplus_fading,
):
    seqs = predecessor_index.shape[0]
    heads = increment_offset.shape[0]
    wx = jnp.transpose(lane_feed_matrix, (1, 2, 3, 0)).reshape(heads * HD, D)
    wz = jnp.transpose(final_valve_matrix, (1, 2, 3, 0)).reshape(heads * HD, D)
    dt_own = lax.dynamic_slice(
        jnp.transpose(increment_matrix, (1, 2, 0)), (kv_index * heads, tp_index, 0), (heads, 1, D)
    )
    wb = entry_basis_matrix.reshape(D, N)
    wc = readout_basis_matrix.reshape(D, N)
    head_rows = jnp.stack(
        [x.reshape(heads) for x in (increment_offset, shrink_speed_exponent, lane_bypass_factor)]
    )
    ready = prep(
        leading_scaling_factor.reshape(1, D),
        dt_own.reshape(heads, D),
        jnp.transpose(lane_filter_memory, (1, 0, 2, 3, 4)).reshape(WIN, seqs, heads * HD),
        jnp.transpose(entry_basis_memory, (1, 0, 2, 3)).reshape(WIN, seqs, N),
        jnp.transpose(readout_basis_memory, (1, 0, 2, 3)).reshape(WIN, seqs, N),
        lane_feed_kernel,
        entry_basis_kernel,
        readout_basis_kernel,
        head_rows,
        jnp.transpose(predecessor_index),
        admitted_counts.reshape(1, seqs),
        jnp.transpose(surplus_fading, (1, 2, 3, 0)),
        hidden_carried_memory.reshape(seqs, heads * HD, N),
    )
    return (wx, in_hbm(wz), wb, wc, *(in_vmem(x) for x in ready))


def shards(candidate_vectors, leading_scaling_factor, lane_feed_matrix, final_valve_matrix,
           increment_matrix, entry_basis_matrix, readout_basis_matrix, lane_feed_kernel,
           entry_basis_kernel, readout_basis_kernel, increment_offset, shrink_speed_exponent,
           lane_bypass_factor, final_linear_matrix, *memories):
    copies = pack(candidate_vectors, lax.axis_size(KV))
    along = lax.all_to_all(copies, KV, split_axis=0, concat_axis=0, tiled=True)
    pieces = lax.all_gather(along, "tp")
    rest = prepared(
        lax.axis_index(KV), lax.axis_index("tp"), leading_scaling_factor, lane_feed_matrix,
        final_valve_matrix, increment_matrix, entry_basis_matrix, readout_basis_matrix,
        lane_feed_kernel, entry_basis_kernel, readout_basis_kernel, increment_offset,
        shrink_speed_exponent, lane_bypass_factor, *memories,
    )
    gated = mixer(pieces, *rest)
    far = lax.all_gather(gated, "far")
    along = lax.all_gather(far, "near")
    swapped = lax.ppermute(along, "tp", [(0, 1), (1, 0)])
    weight = final_linear_matrix.reshape(HG * G * HD, -1)
    return last(lax.axis_index("tp").reshape(1), along, swapped, weight)


def solution(mesh):
    grp, dp, kv, tp = (mesh.shape[axis] for axis in ("grp", "dp", "kv", "tp"))
    near = 4 if kv % 4 == 0 else 1
    split = Mesh(mesh.devices.reshape(grp, dp, kv // near, near, tp), ("grp", "dp", *KV, "tp"))
    placed = (
        P(("grp", "dp"), None, (*KV, "tp")),
        P(),
        P(None, KV, "tp", None),
        P(None, KV, "tp", None),
        P(),
        P(None, "tp", None),
        P(None, "tp", None),
        P(None, KV, "tp", None),
        P(None, "tp", None),
        P(None, "tp", None),
        P(KV, "tp"),
        P(KV, "tp"),
        P(KV, "tp"),
        P(None, None, None, (*KV, "tp")),
        P(("grp", "dp"), KV, "tp", None, None),
        P(("grp", "dp"), None, KV, "tp", None),
        P(("grp", "dp"), None, "tp", None),
        P(("grp", "dp"), None, "tp", None),
        P(("grp", "dp"), None),
        P(("grp", "dp")),
        P(("grp", "dp"), None, KV, "tp"),
    )
    return jax.shard_map(
        shards,
        mesh=split,
        in_specs=placed,
        out_specs=P(("grp", "dp"), None, (*KV, "tp")),
        check_vma=False,
    )
```

time: 111 us -> 108 us (0.973)
  local copies, waits for them, and re-layouts: 12.8 us -> 4.39 us
  waiting for transfers between devices: 1.52 us -> 8.21 us
  other arithmetic: 6.55 us -> 1.27 us
  blocking collectives: 31.8 us -> 35.4 us
  Pallas kernels: 3.62 us -> 6.14 us
  starting transfers between devices: 53.4 us -> 52.1 us
    all_to_all x1, waiting for transfers between devices: 0.01 us -> 6.7 us  [shards(): along = lax.all_to_all(copies, KV, split_axis=0, concat_axis=0, tiled=True)]
    unnamed x34 -> x13, local copies, waits for them, and re-layouts: 4.84 us -> 1.42 us
    reshape x5 -> x0, local copies, waits for them, and re-layouts: 3.3 us -> none  [the longest x3 1.89 us: per_lane(): return jnp.broadcast_to(values, (heads, HD)).reshape(1, heads * HD)]
    all_gather x1 -> x2, blocking collectives: 25.3 us -> 28 us  [the longest x1 15.1 us: shards(): far = lax.all_gather(gated, 'far')]
    concatenate x3 -> x0, other arithmetic: 2.59 us -> none  [the longest x1 1.3 us: prepared(): jnp.concatenate([lane_feed_kernel.reshape(CONV, heads * HD), entry_basis_...]
    pallas_call x1 -> x2, Pallas kernels: 1.72 us -> 4.22 us  [the longest x1 2.22 us: mixer(): pl.pallas_call(mixer_kernel, out_shape=jax.ShapeDtypeStruct((2 * half, 2...]
    broadcast_in_dim x4 -> x0, local copies, waits for them, and re-layouts: 2.26 us -> none  [the longest x3 1.52 us: per_lane(): return jnp.broadcast_to(values, (heads, HD)).reshape(1, heads * HD)]
    convert_element_type x1 -> x0, other arithmetic: 1.94 us -> none  [prepared(): hidden_carried_memory.reshape(seqs, heads * HD, N).astype(jnp.bfloat16)]
  transfers between devices with their start and end apart: 2 -> 2, of which waited for: 1 -> 2; matrix products, arithmetic and copies ran while one was open for 14% -> 4% of each run, Pallas kernels for 0% -> 2%
where the time goes in v2:
time: 108 us
  starting transfers between devices  52.1 us (48%)
  blocking collectives  35.4 us (33%)
  waiting for transfers between devices  8.21 us (8%)
  Pallas kernels  6.14 us (6%)
  local copies, waits for them, and re-layouts  4.39 us (4%)
  other arithmetic  1.27 us (1%)
    all_to_all x1, starting transfers between devices, shards(): along = lax.all_to_all(copies, KV, split_axis=0, concat_axis=0, tiled=True)  44.4 us
    all_gather x1, blocking collectives, shards(): far = lax.all_gather(gated, 'far')  15.1 us
    all_gather x1, blocking collectives, shards(): along = lax.all_gather(far, 'near')  13 us
    ppermute x1, starting transfers between devices, shards(): swapped = lax.ppermute(along, 'tp', [(0, 1), (1, 0)])  7.78 us
    all_gather x1, blocking collectives, shards(): pieces = lax.all_gather(along, 'tp')  7.33 us
    all_to_all x1, waiting for transfers between devices, shards(): along = lax.all_to_all(copies, KV, split_axis=0, concat_axis=0, tiled=True)  6.7 us
    pallas_call x1, Pallas kernels, mixer(): pl.pallas_call(mixer_kernel, out_shape=jax.ShapeDtypeStruct((2 * half, 2...  2.22 us
  transfers between devices with their start and end apart: 2, of which 2 were waited for; matrix products, arithmetic and copies ran while one was open for 4% of the time, Pallas kernels for 2%

profile of v2, /device:TPU:65, one launch (start us, length us, event | category | flops | bytes accessed | tf_op | source)
XLA Modules:
  0.0 107.6 jit_solution(899969606096444220)
XLA Ops:
  0.0 0.0 copy-start
  0.0 0.0 copy-start.5
  0.0 0.8 copy-done.5
  0.8 0.8 pack.1
  1.6 0.0 copy-start.2
  1.6 0.0 copy-start.3
  1.6 0.0 copy-start.4
  1.6 44.4 %all-to-all-start = ((bf16[16,64,128]{2,1,0:T(8,128)(2,1)}), bf16[16,64,128]{2,1,0:T(8,128)(2,1)S(1)}, u32[]{:S(2)}, u32[]{:S(2)}) async-start(bf16[16,64,128]{2,1,0:T(8,128)(2,1)} %pack.1), calls=%async_computation | async-start | bytes 524288 | tf_op jit(solution)/shard_map/all_to_all | solution.py:439
  46.0 1.3 %reshape.44.refs_0_ = bf16[1,2048]{1,0:T(2,128)(2,1)} reshape(bf16[2048]{0:T(1024)(128)(2,1)} %param.22) | data formatting | bytes 8192 | tf_op jit(solution)/shard_map/reshape | solution.py:417
  47.3 0.0 copy-done
  47.3 0.6 copy.33
  47.9 1.0 reshape.55
  48.9 0.6 copy.30.refs_2_
  49.6 1.3 %pad_maximum_fusion.refs_8_ = f32[3,2]{1,0:T(4,128)} fusion(f32[1,2]{1,0:T(1,128)} %bitcast.55, f32[1,2]{1,0:T(1,128)} %bitcast.56, f32[1,2]{1,0:T(1,128)} %bitcast.57), kind=kLoop, calls=%fused_computation.1 | loop fusion | flops 12 | bytes 48 | tf_op jit(solution)/shard_map/stack | solution.py:413
  50.8 2.0 %prep.1 = (f32[168,128]{1,0:T(8,128)S(1)}, bf16[34,128,128]{2,1,0:T(8,128)(2,1)S(1)}, bf16[416,128]{1,0:T(8,128)(2,1)S(1)}) custom-call(bf16[1,2048]{1,0:T(2,128)(2,1)} %reshape.44.refs_0_, bf16[2,2048]{1,0:T(2,128)(2,1)} %bitcast.51, bf16[7,32,128]{2,1,0:T(8,128)(2,1)} %copy.30.refs_2_, bf16[7,32,128]{2,1,0:T(8,128)(2,1)} %bitcast.49, ...), custom_call_target="tpu_custom_call" | custom-call | flops 16777216 | bytes 4194304 | tf_op jit(solution)/shard_map/prep/pallas_call | solution.py:322
  52.9 6.7 %all-to-all-done = bf16[16,64,128]{2,1,0:T(8,128)(2,1)S(1)} async-done(((bf16[16,64,128]{2,1,0:T(8,128)(2,1)}), bf16[16,64,128]{2,1,0:T(8,128)(2,1)S(1)}, u32[]{:S(2)}, u32[]{:S(2)}) %all-to-all-start) | async-done | bytes 262176 | tf_op jit(solution)/shard_map/all_to_all | solution.py:439
  59.6 7.3 %all-gather = bf16[32,64,128]{2,1,0:T(8,128)(2,1)S(1)} all-gather(bf16[16,64,128]{2,1,0:T(8,128)(2,1)S(1)} %all-to-all-done), channel_id=2, replica_groups=mesh['grp'=2,'dp'=8,'far'=4,'near'=4,'tp'=2] {'tp'}, dimensions={0}, use_global_device_ids=true | all-gather | bytes 786432 | tf_op jit(solution)/shard_map/all_gather | solution.py:440
  66.9 0.0 copy-done.2
  66.9 0.0 copy-done.3
  66.9 0.0 copy-done.4
  66.9 0.0 copy-start.1
  66.9 2.2 %mixer.1 = bf16[128,128]{1,0:T(8,128)(2,1)S(1)} custom-call(bf16[2,16,64,128]{3,2,1,0:T(8,128)(2,1)S(1)} %bitcast.40, bf16[128,2048]{1,0:T(8,128)(2,1)S(1)} %bitcast.42, bf16[128,2048]{1,0:T(8,128)(2,1)} %bitcast.46, bf16[2048,128]{1,0:T(8,128)(2,1)S(1)} %bitcast.43, bf16[2048,128]{1,0:T(8,128)(2,1)S(1)} %bitcast.44, ...), custom_call_target="tpu_custom_call" | custom-call | flops 335544320 | bytes 5242880 | tf_op jit(solution)/shard_map/mixer/pallas_call | solution.py:342
  69.1 15.1 %all-gather.1 = bf16[512,128]{1,0:T(8,128)(2,1)S(1)} all-gather(bf16[128,128]{1,0:T(8,128)(2,1)S(1)} %mixer.1), channel_id=3, replica_groups=mesh['grp'=2,'dp'=8,'far'=4,'near'=4,'tp'=2] {'far'}, dimensions={0}, use_global_device_ids=true | all-gather | bytes 163840 | tf_op jit(solution)/shard_map/all_gather | solution.py:448
  84.2 13.0 %all-gather.2 = bf16[16,128,128]{2,1,0:T(8,128)(2,1)S(1)} all-gather(bf16[4,128,128]{2,1,0:T(8,128)(2,1)S(1)} %bitcast.47), channel_id=4, replica_groups=mesh['grp'=2,'dp'=8,'far'=4,'near'=4,'tp'=2] {'near'}, dimensions={0}, use_global_device_ids=true | all-gather | bytes 655360 | tf_op jit(solution)/shard_map/all_gather | solution.py:449
  97.2 7.8 %collective-permute-start = (bf16[4,4,128,128]{3,2,1,0:T(8,128)(2,1)S(1)}, bf16[4,4,128,128]{3,2,1,0:T(8,128)(2,1)S(1)}, u32[]{:S(2)}, u32[]{:S(2)}) collective-permute-start(bf16[4,4,128,128]{3,2,1,0:T(8,128)(2,1)S(1)} %bitcast.38), channel_id=1, source_target_pairs={{0,1},{1,0},{2,3},{3,2},{4,5},{5,4},{6,7},{7,6},{8,9},{9,8},{10,11... | collective-permute-start | bytes 1572872 | tf_op jit(solution)/shard_map/ppermute | solution.py:450
  105.0 1.5 %collective-permute-done.other_ref = bf16[4,4,128,128]{3,2,1,0:T(8,128)(2,1)S(1)} collective-permute-done((bf16[4,4,128,128]{3,2,1,0:T(8,128)(2,1)S(1)}, bf16[4,4,128,128]{3,2,1,0:T(8,128)(2,1)S(1)}, u32[]{:S(2)}, u32[]{:S(2)}) %collective-permute-start) | collective-permute-done | bytes 524320 | tf_op jit(solution)/shard_map/ppermute | solution.py:450
  106.5 0.0 copy-done.1
  106.5 1.1 %last.1 = bf16[32,4,64]{2,1,0:T(4,128)(2,1)} custom-call(s32[1]{0:T(128)} %bitcast.tp_ref, bf16[4,4,128,128]{3,2,1,0:T(8,128)(2,1)S(1)} %bitcast.39, bf16[4,4,128,128]{3,2,1,0:T(8,128)(2,1)S(1)} %collective-permute-done.other_ref, bf16[4096,64]{1,0:T(8,128)(2,1)S(1)} %bitcast.41), custom_call_target="tpu_custom_call" | custom-call | flops 67108864 | bytes 2097152 | tf_op jit(solution)/shard_map/last/pallas_call | solution.py:366
  (1 shorter events, 0.0 us)
Async XLA Ops:
  0.0 47.3 %copy-start = (bf16[2048,32,2]{0,2,1:T(2,128)(2,1)S(1)}, bf16[2048,32,2]{0,2,1:T(2,128)(2,1)}, u32[]{:S(2)}) copy-start(bf16[2048,32,2]{0,2,1:T(2,128)(2,1)} %param.25) | copy-start | bytes 786436
  0.0 0.8 copy-start.5
  1.6 65.3 %copy-start.2 = (bf16[2048,2,1,64]{0,3,2,1:T(8,128)(2,1)S(1)}, bf16[2048,2,1,64]{0,3,2,1:T(8,128)(2,1)}, u32[]{:S(2)}) copy-start(bf16[2048,2,1,64]{0,3,2,1:T(8,128)(2,1)} %param.23) | copy-start | bytes 1572868
  1.6 65.3 %copy-start.3 = (bf16[2048,1,128]{2,0,1:T(8,128)(2,1)S(1)}, bf16[2048,1,128]{2,0,1:T(8,128)(2,1)}, u32[]{:S(2)}) copy-start(bf16[2048,1,128]{2,0,1:T(8,128)(2,1)} %param.26) | copy-start | bytes 1572868
  1.6 65.3 %copy-start.4 = (bf16[2048,1,128]{2,0,1:T(8,128)(2,1)S(1)}, bf16[2048,1,128]{2,0,1:T(8,128)(2,1)}, u32[]{:S(2)}) copy-start(bf16[2048,1,128]{2,0,1:T(8,128)(2,1)} %param.27) | copy-start | bytes 1572868
  1.6 57.9 %all-to-all-start = ((bf16[16,64,128]{2,1,0:T(8,128)(2,1)}), bf16[16,64,128]{2,1,0:T(8,128)(2,1)S(1)}, u32[]{:S(2)}, u32[]{:S(2)}) async-start(bf16[16,64,128]{2,1,0:T(8,128)(2,1)} %pack.1), calls=%async_computation | async-start | bytes 524288 | tf_op jit(solution)/shard_map/all_to_all | solution.py:439
  66.9 39.6 %copy-start.1 = (bf16[32,2,64,64]{3,2,1,0:T(8,128)(2,1)S(1)}, bf16[32,2,64,64]{3,2,1,0:T(8,128)(2,1)}, u32[]{:S(2)}) copy-start(bf16[32,2,64,64]{3,2,1,0:T(8,128)(2,1)} %param.34) | copy-start | bytes 1572868
  97.2 9.3 %collective-permute-start = (bf16[4,4,128,128]{3,2,1,0:T(8,128)(2,1)S(1)}, bf16[4,4,128,128]{3,2,1,0:T(8,128)(2,1)S(1)}, u32[]{:S(2)}, u32[]{:S(2)}) collective-permute-start(bf16[4,4,128,128]{3,2,1,0:T(8,128)(2,1)S(1)} %bitcast.38), channel_id=1, source_target_pairs={{0,1},{1,0},{2,3},{3,2},{4,5},{5,4},{6,7},{7,6},{8,9},{9,8},{10,11... | collective-permute-start | bytes 1572872 | tf_op jit(solution)/shard_map/ppermute | solution.py:450

commit v3 on v2

--- a/solution.py
+++ b/solution.py
@@ -5,7 +5,6 @@
 from jax import lax
 from jax.experimental import pallas as pl
 from jax.experimental.pallas import tpu as pltpu
-from jax.sharding import Mesh
 from jax.sharding import PartitionSpec as P
 
 D = 2048
@@ -18,7 +17,7 @@
 PROP = 4
 PREV = 4
 
-KV = ("far", "near")
+KV = "kv"
 
 INTERPRET = False
 
@@ -52,7 +51,7 @@
 
 def places(seqs):
     at, row = {}, 0
-    sizes = (("gain", D // N), ("taps", 16), ("heads", 8), ("fading", PROP * seqs), ("end", 0))
+    sizes = (("taps", 16), ("heads", 8), ("fading", PROP * seqs), ("end", 0))
     for name, size in sizes:
         at[name] = row
         row += size
@@ -91,7 +90,6 @@
         wide_out[start : start + value.shape[0], :] = value
 
     for k in range(D // N):
-        put("gain", k, gain_ref[:, k * N : (k + 1) * N].astype(f32))
         pair = [
             jnp.broadcast_to(dt_ref[h : h + 1, k * N : (k + 1) * N].astype(f32), (8, N))
             for h in range(2)
@@ -100,6 +98,8 @@
         narrow_out[seqs + k // 8, row : row + 16, :] = jnp.concatenate(pair, axis=0).astype(
             jnp.bfloat16
         )
+    gains = [gain_ref[:, k * N : (k + 1) * N].astype(f32) for k in range(D // N)]
+    narrow_out[seqs + D // N // 8, : D // N, :] = jnp.concatenate(gains, axis=0).astype(jnp.bfloat16)
     for t in range(CONV):
         put("taps", t, jnp.concatenate([taps_x_ref[t, h] for h in range(2)], axis=1))
         put("taps", CONV + t, taps_b_ref[t])
@@ -149,28 +149,34 @@
     wz_ref,
     wb_ref,
     wc_ref,
-    wide_ref,
     narrow_ref,
-    recent_ref,
+    wide_far,
+    recent_far,
     out_ref,
     cc_all,
     read_all,
-    wz_held,
-    wz_sem,
+    wide_ref,
+    recent_ref,
+    sems,
 ):
     half = pieces_ref.shape[2]
     seqs = half // 2
     rows = 2 * half
     kv_count = pieces_ref.shape[1]
     f32 = jnp.float32
-    wz_copy = pltpu.make_async_copy(wz_ref, wz_held, wz_sem)
-    wz_copy.start()
+    copies = [
+        pltpu.make_async_copy(wide_far, wide_ref, sems.at[0]),
+        pltpu.make_async_copy(recent_far, recent_ref, sems.at[1]),
+    ]
+    for copy in copies:
+        copy.start()
     left = lax.broadcasted_iota(jnp.int32, (half, 2 * HD), 1) < HD
     at = places(seqs)
 
     def table(name, index, size):
         return wide_ref[at[name] + index * size : at[name] + (index + 1) * size, :]
 
+    gains = narrow_ref[seqs + D // N // 8, : D // N, :].astype(f32)
     scaled = []
     square = jnp.zeros((rows, 2 * HD), f32)
     for k in range(kv_count):
@@ -180,7 +186,7 @@
         low = jnp.where(left, pltpu.roll(p0, HD, 1), p1)
         both = jnp.concatenate([top, low], axis=0)
         square = square + both * both
-        gain = table("gain", k, 1)
+        gain = gains[k : k + 1, :]
         scaled.append((both * gain).astype(jnp.bfloat16))
     u = jnp.concatenate(scaled, axis=1)
     r_in = lax.rsqrt(jnp.sum(square, axis=1, keepdims=True) / D + 1e-06)
@@ -193,12 +199,16 @@
     c_rows = times(wc_ref[...], down).astype(jnp.bfloat16).astype(f32)
     b_rows = times(wb_ref[...], down).astype(jnp.bfloat16).astype(f32)
     x_rows = times(wx_ref[...], across).astype(jnp.bfloat16).astype(f32)
+    z_rows = times(wz_ref[...], across).astype(jnp.bfloat16).astype(f32)
     chunks = [narrow_ref[seqs + k // 8, (k % 8) * 16 : (k % 8) * 16 + 16, :] for k in range(D // N)]
     dt_cols = times(jnp.concatenate(chunks, axis=1), across)
     dt_raw = jnp.where(
         lax.broadcasted_iota(jnp.int32, (rows, 2 * HD), 1) < HD,
         *(jnp.broadcast_to(dt_cols[:, c : c + 1], (rows, 2 * HD)) for c in (0, 8)),
     )
+
+    for copy in copies:
+        copy.wait()
 
     def recent(index):
         return recent_ref[index * seqs : (index + 1) * seqs, :].astype(f32)
@@ -259,8 +269,6 @@
                 reach = reach | (child[j][p] & above[p][i])
             line.append(reach)
         above.append(line)
-    wz_copy.wait()
-    z_rows = times(wz_held[...], across).astype(jnp.bfloat16).astype(f32)
     for j in range(PROP):
         y = jnp.exp(level[j]) * read_all[:, j, :] + bypass * xc[j]
         for i in range(j + 1):
@@ -276,16 +284,16 @@
 
 def last_kernel(tp_ref, own_ref, other_ref, weight_ref, out_ref, spread):
     f32 = jnp.float32
-    near, far, rows = own_ref.shape[:3]
+    kv_count, rows = own_ref.shape[:2]
     seqs = rows // PROP
     group = tp_ref[0]
     total = jnp.zeros((rows, weight_ref.shape[1]), f32)
     square = jnp.zeros((rows, 2 * HD), f32)
-    for k in range(near * far):
+    for k in range(kv_count):
         lhs = []
         rhs = []
         for ref, t in ((own_ref, group), (other_ref, 1 - group)):
-            piece = ref[k % near, k // near]
+            piece = ref[k]
             wide = piece.astype(f32)
             square = square + wide * wide
             lhs.append(piece)
@@ -322,9 +330,9 @@
     return pl.pallas_call(
         prep_kernel,
         out_shape=[
-            pltpu.VMEM((places(seqs)["end"], N), jnp.float32),
-            pltpu.VMEM((seqs + D // N // 8, N, N), jnp.bfloat16),
-            pltpu.VMEM(((3 * (CONV - 1) + PROP) * seqs, N), jnp.bfloat16),
+            jax.ShapeDtypeStruct((places(seqs)["end"], N), jnp.float32),
+            pltpu.VMEM((seqs + D // N // 8 + 1, N, N), jnp.bfloat16),
+            jax.ShapeDtypeStruct(((3 * (CONV - 1) + PROP) * seqs, N), jnp.bfloat16),
         ],
         in_specs=[pl.BlockSpec(memory_space=pltpu.HBM)] * len(inputs),
         out_specs=vmem(3),
@@ -342,13 +350,13 @@
     return pl.pallas_call(
         mixer_kernel,
         out_shape=jax.ShapeDtypeStruct((2 * half, 2 * HD), jnp.bfloat16),
-        in_specs=vmem(2) + [pl.BlockSpec(memory_space=pltpu.HBM)] + vmem(len(rest) - 2),
+        in_specs=vmem(6) + [pl.BlockSpec(memory_space=pltpu.HBM)] * 2,
         out_specs=vmem(1)[0],
         scratch_shapes=[
             pltpu.VMEM((half // 2, 2 * PROP, N), jnp.float32),
             pltpu.VMEM((half // 2, 2 * PROP, 2 * HD), jnp.float32),
-            pltpu.VMEM((2 * HD, D), jnp.bfloat16),
-            pltpu.SemaphoreType.DMA,
+            *(pltpu.VMEM(x.shape, x.dtype) for x in rest[-2:]),
+            pltpu.SemaphoreType.DMA((2,)),
         ],
         compiler_params=pltpu.CompilerParams(vmem_limit_bytes=20 << 20),
         cost_estimate=pl.CostEstimate(
@@ -360,7 +368,7 @@
 
 
 def last(group, own, other, weight):
-    rows = own.shape[2]
+    rows = own.shape[1]
     seqs = rows // PROP
     cols = weight.shape[1]
     return pl.pallas_call(
@@ -413,7 +421,7 @@
     head_rows = jnp.stack(
         [x.reshape(heads) for x in (increment_offset, shrink_speed_exponent, lane_bypass_factor)]
     )
-    ready = prep(
+    wide, narrow, recent = prep(
         leading_scaling_factor.reshape(1, D),
         dt_own.reshape(heads, D),
         jnp.transpose(lane_filter_memory, (1, 0, 2, 3, 4)).reshape(WIN, seqs, heads * HD),
@@ -428,7 +436,7 @@
         jnp.transpose(surplus_fading, (1, 2, 3, 0)),
         hidden_carried_memory.reshape(seqs, heads * HD, N),
     )
-    return (wx, in_hbm(wz), wb, wc, *(in_vmem(x) for x in ready))
+    return (wx, wz, wb, wc, in_vmem(narrow), in_hbm(wide), in_hbm(recent))
 
 
 def shards(candidate_vectors, leading_scaling_factor, lane_feed_matrix, final_valve_matrix,
@@ -445,19 +453,15 @@
         shrink_speed_exponent, lane_bypass_factor, *memories,
     )
     gated = mixer(pieces, *rest)
-    far = lax.all_gather(gated, "far")
-    along = lax.all_gather(far, "near")
+    along = lax.all_gather(gated, KV)
     swapped = lax.ppermute(along, "tp", [(0, 1), (1, 0)])
     weight = final_linear_matrix.reshape(HG * G * HD, -1)
     return last(lax.axis_index("tp").reshape(1), along, swapped, weight)
 
 
 def solution(mesh):
-    grp, dp, kv, tp = (mesh.shape[axis] for axis in ("grp", "dp", "kv", "tp"))
-    near = 4 if kv % 4 == 0 else 1
-    split = Mesh(mesh.devices.reshape(grp, dp, kv // near, near, tp), ("grp", "dp", *KV, "tp"))
     placed = (
-        P(("grp", "dp"), None, (*KV, "tp")),
+        P(("grp", "dp"), None, ("kv", "tp")),
         P(),
         P(None, KV, "tp", None),
         P(None, KV, "tp", None),
@@ -470,7 +474,7 @@
         P(KV, "tp"),
         P(KV, "tp"),
         P(KV, "tp"),
-        P(None, None, None, (*KV, "tp")),
+        P(None, None, None, ("kv", "tp")),
         P(("grp", "dp"), KV, "tp", None, None),
         P(("grp", "dp"), None, KV, "tp", None),
         P(("grp", "dp"), None, "tp", None),
@@ -481,8 +485,8 @@
     )
     return jax.shard_map(
         shards,
-        mesh=split,
+        mesh=mesh,
         in_specs=placed,
-        out_specs=P(("grp", "dp"), None, (*KV, "tp")),
+        out_specs=P(("grp", "dp"), None, ("kv", "tp")),
         check_vma=False,
     )

time: 108 us -> 108 us (level)
  waiting for transfers between devices: 8.21 us -> 5.99 us
  starting transfers between devices: 52.1 us -> 53.6 us
  local copies, waits for them, and re-layouts: 4.39 us -> 5.67 us
  blocking collectives: 35.4 us -> 34.2 us
    all_gather x2 -> x1, blocking collectives: 28 us -> 25.3 us  [shards(): along = lax.all_gather(gated, KV)]
    all_to_all x1, waiting for transfers between devices: 6.7 us -> 4.48 us  [shards(): along = lax.all_to_all(copies, KV, split_axis=0, concat_axis=0, tiled=True)]
    all_gather x1, blocking collectives: 7.33 us -> 8.9 us  [shards(): pieces = lax.all_gather(along, 'tp')]
    ppermute x1, starting transfers between devices: 7.78 us -> 9.22 us  [shards(): swapped = lax.ppermute(along, 'tp', [(0, 1), (1, 0)])]
    unnamed x13 -> x19, local copies, waits for them, and re-layouts: 1.42 us -> 2.7 us
  transfers between devices with their start and end apart: 2 -> 2, of which waited for: 2 -> 2; matrix products, arithmetic and copies ran while one was open for 4% -> 5% of each run, Pallas kernels for 2% -> 2%
where the time goes in v3:
time: 108 us; the launch traced here: 107 us
  starting transfers between devices  53.6 us (50%)
  blocking collectives  34.2 us (32%)
  Pallas kernels  6.34 us (6%)
  waiting for transfers between devices  5.99 us (6%)
  local copies, waits for them, and re-layouts  5.67 us (5%)
  other arithmetic  1.26 us (1%)
    all_to_all x1, starting transfers between devices, shards(): along = lax.all_to_all(copies, KV, split_axis=0, concat_axis=0, tiled=True)  44.4 us
    all_gather x1, blocking collectives, shards(): along = lax.all_gather(gated, KV)  25.3 us
    ppermute x1, starting transfers between devices, shards(): swapped = lax.ppermute(along, 'tp', [(0, 1), (1, 0)])  9.22 us
    all_gather x1, blocking collectives, shards(): pieces = lax.all_gather(along, 'tp')  8.9 us
    all_to_all x1, waiting for transfers between devices, shards(): along = lax.all_to_all(copies, KV, split_axis=0, concat_axis=0, tiled=True)  4.48 us
    unnamed x19, local copies, waits for them, and re-layouts  2.7 us
    pallas_call x1, Pallas kernels, mixer(): pl.pallas_call(mixer_kernel, out_shape=jax.ShapeDtypeStruct((2 * half, 2...  2.39 us
  transfers between devices with their start and end apart: 2, of which 2 were waited for; matrix products, arithmetic and copies ran while one was open for 5% of the time, Pallas kernels for 2%

profile of v3, /device:TPU:65, one launch (start us, length us, event | category | flops | bytes accessed | tf_op | source)
XLA Modules:
  0.0 107.2 jit_solution(10950947595621526301)
XLA Ops:
  0.0 0.0 copy-start
  0.0 0.0 copy-start.8
  0.0 0.8 copy-done.8
  0.8 0.8 pack.1
  1.6 0.0 copy-start.2
  1.6 0.0 copy-start.3
  1.6 0.0 copy-start.4
  1.6 0.0 copy-start.5
  1.7 44.4 %all-to-all-start = ((bf16[16,64,128]{2,1,0:T(8,128)(2,1)}), bf16[16,64,128]{2,1,0:T(8,128)(2,1)}, u32[]{:S(2)}, u32[]{:S(2)}) async-start(bf16[16,64,128]{2,1,0:T(8,128)(2,1)} %pack.1), calls=%async_computation | async-start | bytes 524288 | tf_op jit(solution)/shard_map/all_to_all | solution.py:447
  46.0 1.3 %reshape.44.refs_0_ = bf16[1,2048]{1,0:T(2,128)(2,1)} reshape(bf16[2048]{0:T(1024)(128)(2,1)} %param.22) | data formatting | bytes 8192 | tf_op jit(solution)/shard_map/reshape | solution.py:425
  47.3 0.0 copy-done
  47.4 0.6 copy.33
  48.0 1.0 reshape.54
  49.0 0.6 copy.30.refs_2_
  49.6 1.3 %pad_maximum_fusion.refs_8_ = f32[3,2]{1,0:T(4,128)} fusion(f32[1,2]{1,0:T(1,128)} %bitcast.53, f32[1,2]{1,0:T(1,128)} %bitcast.54, f32[1,2]{1,0:T(1,128)} %bitcast.55), kind=kLoop, calls=%fused_computation.1 | loop fusion | flops 12 | bytes 48 | tf_op jit(solution)/shard_map/stack | solution.py:421
  50.9 2.0 %prep.1 = (f32[152,128]{1,0:T(8,128)S(1)}, bf16[35,128,128]{2,1,0:T(8,128)(2,1)S(1)}, bf16[416,128]{1,0:T(8,128)(2,1)S(1)}) custom-call(bf16[1,2048]{1,0:T(2,128)(2,1)} %reshape.44.refs_0_, bf16[2,2048]{1,0:T(2,128)(2,1)} %bitcast.49, bf16[7,32,128]{2,1,0:T(8,128)(2,1)} %copy.30.refs_2_, bf16[7,32,128]{2,1,0:T(8,128)(2,1)} %bitcast.47, ...), custom_call_target="tpu_custom_call" | custom-call | flops 16777216 | bytes 4194304 | tf_op jit(solution)/shard_map/prep/pallas_call | solution.py:330
  52.9 0.0 copy-start.6
  52.9 0.6 copy-done.6
  53.5 0.0 copy-start.7
  53.5 0.6 copy-done.7
  54.2 4.5 %all-to-all-done = bf16[16,64,128]{2,1,0:T(8,128)(2,1)} async-done(((bf16[16,64,128]{2,1,0:T(8,128)(2,1)}), bf16[16,64,128]{2,1,0:T(8,128)(2,1)}, u32[]{:S(2)}, u32[]{:S(2)}) %all-to-all-start) | async-done | bytes 262176 | tf_op jit(solution)/shard_map/all_to_all | solution.py:447
  58.6 8.9 %all-gather = bf16[32,64,128]{2,1,0:T(8,128)(2,1)S(1)} all-gather(bf16[16,64,128]{2,1,0:T(8,128)(2,1)} %all-to-all-done), channel_id=2, replica_groups=mesh['grp'=2,'dp'=8,'kv'=16,'tp'=2] {'tp'}, dimensions={0}, use_global_device_ids=true | all-gather | bytes 786432 | tf_op jit(solution)/shard_map/all_gather | solution.py:448
  67.5 0.0 copy-done.2
  67.5 0.0 copy-done.3
  67.5 0.0 copy-done.4
  67.6 0.0 copy-done.5
  67.6 0.0 copy-start.1
  67.6 2.4 %mixer.1 = bf16[128,128]{1,0:T(8,128)(2,1)S(1)} custom-call(bf16[2,16,64,128]{3,2,1,0:T(8,128)(2,1)S(1)} %bitcast.39, bf16[128,2048]{1,0:T(8,128)(2,1)S(1)} %bitcast.41, bf16[128,2048]{1,0:T(8,128)(2,1)S(1)} %bitcast.42, bf16[2048,128]{1,0:T(8,128)(2,1)S(1)} %bitcast.43, bf16[2048,128]{1,0:T(8,128)(2,1)S(1)} %bitcast.44, ...), custom_call_target="tpu_custom_call" | custom-call | flops 335544320 | bytes 5242880 | tf_op jit(solution)/shard_map/mixer/pallas_call | solution.py:350
  70.0 25.3 %all-gather.1 = bf16[2048,128]{1,0:T(8,128)(2,1)S(1)} all-gather(bf16[128,128]{1,0:T(8,128)(2,1)S(1)} %mixer.1), channel_id=3, replica_groups=mesh['grp'=2,'dp'=8,'kv'=16,'tp'=2] {'kv'}, dimensions={0}, use_global_device_ids=true | all-gather | bytes 557056 | tf_op jit(solution)/shard_map/all_gather | solution.py:456
  95.3 9.2 %collective-permute-start = (bf16[16,128,128]{2,1,0:T(8,128)(2,1)S(1)}, bf16[16,128,128]{2,1,0:T(8,128)(2,1)S(1)}, u32[]{:S(2)}, u32[]{:S(2)}) collective-permute-start(bf16[16,128,128]{2,1,0:T(8,128)(2,1)S(1)} %bitcast.37), channel_id=1, source_target_pairs={{0,1},{1,0},{2,3},{3,2},{4,5},{5,4},{6,7},{7,6},{8,9},{9,8},{10,11... | collective-permute-start | bytes 1572872 | tf_op jit(solution)/shard_map/ppermute | solution.py:457
  104.5 1.5 %collective-permute-done.other_ref = bf16[16,128,128]{2,1,0:T(8,128)(2,1)S(1)} collective-permute-done((bf16[16,128,128]{2,1,0:T(8,128)(2,1)S(1)}, bf16[16,128,128]{2,1,0:T(8,128)(2,1)S(1)}, u32[]{:S(2)}, u32[]{:S(2)}) %collective-permute-start) | collective-permute-done | bytes 524320 | tf_op jit(solution)/shard_map/ppermute | solution.py:457
  106.1 0.0 copy-done.1
  106.1 1.1 %last.1 = bf16[32,4,64]{2,1,0:T(4,128)(2,1)} custom-call(s32[1]{0:T(128)} %bitcast.tp_ref, bf16[16,128,128]{2,1,0:T(8,128)(2,1)S(1)} %bitcast.38, bf16[16,128,128]{2,1,0:T(8,128)(2,1)S(1)} %collective-permute-done.other_ref, bf16[4096,64]{1,0:T(8,128)(2,1)S(1)} %bitcast.40), custom_call_target="tpu_custom_call" | custom-call | flops 67108864 | bytes 2097152 | tf_op jit(solution)/shard_map/last/pallas_call | solution.py:374
  (1 shorter events, 0.0 us)
Async XLA Ops:
  0.0 47.3 %copy-start = (bf16[2048,32,2]{0,2,1:T(2,128)(2,1)S(1)}, bf16[2048,32,2]{0,2,1:T(2,128)(2,1)}, u32[]{:S(2)}) copy-start(bf16[2048,32,2]{0,2,1:T(2,128)(2,1)} %param.25) | copy-start | bytes 786436
  0.0 0.8 copy-start.8
  1.6 65.9 %copy-start.2 = (bf16[2048,2,1,64]{0,3,2,1:T(8,128)(2,1)S(1)}, bf16[2048,2,1,64]{0,3,2,1:T(8,128)(2,1)}, u32[]{:S(2)}) copy-start(bf16[2048,2,1,64]{0,3,2,1:T(8,128)(2,1)} %param.23) | copy-start | bytes 1572868
  1.6 65.9 %copy-start.3 = (bf16[2048,2,1,64]{0,3,2,1:T(8,128)(2,1)S(1)}, bf16[2048,2,1,64]{0,3,2,1:T(8,128)(2,1)}, u32[]{:S(2)}) copy-start(bf16[2048,2,1,64]{0,3,2,1:T(8,128)(2,1)} %param.24) | copy-start | bytes 1572868
  1.6 65.9 %copy-start.4 = (bf16[2048,1,128]{2,0,1:T(8,128)(2,1)S(1)}, bf16[2048,1,128]{2,0,1:T(8,128)(2,1)}, u32[]{:S(2)}) copy-start(bf16[2048,1,128]{2,0,1:T(8,128)(2,1)} %param.26) | copy-start | bytes 1572868
  1.6 65.9 %copy-start.5 = (bf16[2048,1,128]{2,0,1:T(8,128)(2,1)S(1)}, bf16[2048,1,128]{2,0,1:T(8,128)(2,1)}, u32[]{:S(2)}) copy-start(bf16[2048,1,128]{2,0,1:T(8,128)(2,1)} %param.27) | copy-start | bytes 1572868
  1.7 57.0 %all-to-all-start = ((bf16[16,64,128]{2,1,0:T(8,128)(2,1)}), bf16[16,64,128]{2,1,0:T(8,128)(2,1)}, u32[]{:S(2)}, u32[]{:S(2)}) async-start(bf16[16,64,128]{2,1,0:T(8,128)(2,1)} %pack.1), calls=%async_computation | async-start | bytes 524288 | tf_op jit(solution)/shard_map/all_to_all | solution.py:447
  52.9 0.6 copy-start.6
  53.5 0.6 copy-start.7
  67.6 38.5 %copy-start.1 = (bf16[32,2,64,64]{3,2,1,0:T(8,128)(2,1)S(1)}, bf16[32,2,64,64]{3,2,1,0:T(8,128)(2,1)}, u32[]{:S(2)}) copy-start(bf16[32,2,64,64]{3,2,1,0:T(8,128)(2,1)} %param.34) | copy-start | bytes 1572868
  95.3 10.7 %collective-permute-start = (bf16[16,128,128]{2,1,0:T(8,128)(2,1)S(1)}, bf16[16,128,128]{2,1,0:T(8,128)(2,1)S(1)}, u32[]{:S(2)}, u32[]{:S(2)}) collective-permute-start(bf16[16,128,128]{2,1,0:T(8,128)(2,1)S(1)} %bitcast.37), channel_id=1, source_target_pairs={{0,1},{1,0},{2,3},{3,2},{4,5},{5,4},{6,7},{7,6},{8,9},{9,8},{10,11... | collective-permute-start | bytes 1572872 | tf_op jit(solution)/shard_map/ppermute | solution.py:457

commit v4 on v3

--- a/solution.py
+++ b/solution.py
@@ -32,6 +32,10 @@
 
 def in_hbm(x):
     return x if INTERPRET else pltpu.with_memory_space_constraint(x, pltpu.HBM)
+
+
+def hbm(count):
+    return [pl.BlockSpec(memory_space=pltpu.HBM)] * count
 
 
 def pack_kernel(rows_ref, out_ref, wide):
@@ -146,8 +150,8 @@
 def mixer_kernel(
     pieces_ref,
     wx_ref,
-    wz_ref,
-    wb_ref,
+    wz_far,
+    wb_far,
     wc_ref,
     narrow_ref,
     wide_far,
@@ -157,6 +161,8 @@
     read_all,
     wide_ref,
     recent_ref,
+    wz_ref,
+    wb_ref,
     sems,
 ):
     half = pieces_ref.shape[2]
@@ -167,6 +173,8 @@
     copies = [
         pltpu.make_async_copy(wide_far, wide_ref, sems.at[0]),
         pltpu.make_async_copy(recent_far, recent_ref, sems.at[1]),
+        pltpu.make_async_copy(wb_far, wb_ref, sems.at[2]),
+        pltpu.make_async_copy(wz_far, wz_ref, sems.at[3]),
     ]
     for copy in copies:
         copy.start()
@@ -197,9 +205,7 @@
     across = (((1,), (1,)), ((), ()))
     down = (((1,), (0,)), ((), ()))
     c_rows = times(wc_ref[...], down).astype(jnp.bfloat16).astype(f32)
-    b_rows = times(wb_ref[...], down).astype(jnp.bfloat16).astype(f32)
     x_rows = times(wx_ref[...], across).astype(jnp.bfloat16).astype(f32)
-    z_rows = times(wz_ref[...], across).astype(jnp.bfloat16).astype(f32)
     chunks = [narrow_ref[seqs + k // 8, (k % 8) * 16 : (k % 8) * 16 + 16, :] for k in range(D // N)]
     dt_cols = times(jnp.concatenate(chunks, axis=1), across)
     dt_raw = jnp.where(
@@ -209,6 +215,8 @@
 
     for copy in copies:
         copy.wait()
+    b_rows = times(wb_ref[...], down).astype(jnp.bfloat16).astype(f32)
+    z_rows = times(wz_ref[...], across).astype(jnp.bfloat16).astype(f32)
 
     def recent(index):
         return recent_ref[index * seqs : (index + 1) * seqs, :].astype(f32)
@@ -282,29 +290,39 @@
         out_ref[j * seqs : (j + 1) * seqs, :] = gated
 
 
-def last_kernel(tp_ref, own_ref, other_ref, weight_ref, out_ref, spread):
+def share_of(pieces_ref, first, weight_ref):
     f32 = jnp.float32
-    kv_count, rows = own_ref.shape[:2]
-    seqs = rows // PROP
-    group = tp_ref[0]
+    kv_count, rows = pieces_ref.shape[:2]
     total = jnp.zeros((rows, weight_ref.shape[1]), f32)
     square = jnp.zeros((rows, 2 * HD), f32)
-    for k in range(kv_count):
+    for k in range(0, kv_count, 2):
         lhs = []
         rhs = []
-        for ref, t in ((own_ref, group), (other_ref, 1 - group)):
-            piece = ref[k]
+        for step in range(2):
+            piece = pieces_ref[k + step]
             wide = piece.astype(f32)
             square = square + wide * wide
             lhs.append(piece)
+            core = first if step == 0 else 1 - first
             for h in range(2):
-                start = pl.multiple_of(((2 * k + h) * G + t) * HD, HD)
+                start = pl.multiple_of(((2 * (k + step) + h) * G + core) * HD, HD)
                 rhs.append(weight_ref[pl.ds(start, HD), :])
         total = total + jnp.dot(
             jnp.concatenate(lhs, axis=1), jnp.concatenate(rhs, axis=0), preferred_element_type=f32
         )
-    r_out = lax.rsqrt(jnp.sum(square, axis=1, keepdims=True) / (HG * G * HD) + 1e-05)
-    mixed = total * r_out
+    return total, square
+
+
+def own_kernel(first_ref, pieces_ref, weight_ref, total_ref, square_ref):
+    total_ref[...], square_ref[...] = share_of(pieces_ref, first_ref[0], weight_ref)
+
+
+def last_kernel(first_ref, pieces_ref, weight_ref, total_ref, square_ref, out_ref, spread):
+    rows = pieces_ref.shape[1]
+    seqs = rows // PROP
+    total, square = share_of(pieces_ref, 1 - first_ref[0], weight_ref)
+    square = jnp.sum(square + square_ref[...], axis=1, keepdims=True)
+    mixed = (total + total_ref[...]) * lax.rsqrt(square / (HG * G * HD) + 1e-05)
     for j in range(PROP):
         spread[:, j, :] = mixed[j * seqs : (j + 1) * seqs]
     out_ref[...] = spread[...].astype(jnp.bfloat16)
@@ -350,13 +368,13 @@
     return pl.pallas_call(
         mixer_kernel,
         out_shape=jax.ShapeDtypeStruct((2 * half, 2 * HD), jnp.bfloat16),
-        in_specs=vmem(6) + [pl.BlockSpec(memory_space=pltpu.HBM)] * 2,
+        in_specs=vmem(2) + hbm(2) + vmem(2) + hbm(2),
         out_specs=vmem(1)[0],
         scratch_shapes=[
             pltpu.VMEM((half // 2, 2 * PROP, N), jnp.float32),
             pltpu.VMEM((half // 2, 2 * PROP, 2 * HD), jnp.float32),
-            *(pltpu.VMEM(x.shape, x.dtype) for x in rest[-2:]),
-            pltpu.SemaphoreType.DMA((2,)),
+            *(pltpu.VMEM(x.shape, x.dtype) for x in (rest[-2], rest[-1], rest[1], rest[2])),
+            pltpu.SemaphoreType.DMA((4,)),
         ],
         compiler_params=pltpu.CompilerParams(vmem_limit_bytes=20 << 20),
         cost_estimate=pl.CostEstimate(
@@ -367,23 +385,45 @@
     )(pieces, *rest)
 
 
-def last(group, own, other, weight):
-    rows = own.shape[1]
+def cost_of(pieces, weight):
+    kv_count, rows, width = pieces.shape
+    return pl.CostEstimate(
+        flops=2 * rows * kv_count * width * weight.shape[1], bytes_accessed=1 << 20, transcendentals=rows
+    )
+
+
+def own_half(first, pieces, weight):
+    rows = pieces.shape[1]
+    return pl.pallas_call(
+        own_kernel,
+        out_shape=[
+            jax.ShapeDtypeStruct((rows, weight.shape[1]), jnp.float32),
+            jax.ShapeDtypeStruct((rows, 2 * HD), jnp.float32),
+        ],
+        in_specs=[pl.BlockSpec(memory_space=pltpu.SMEM)] + vmem(2),
+        out_specs=vmem(2),
+        compiler_params=pltpu.CompilerParams(vmem_limit_bytes=16 << 20),
+        cost_estimate=cost_of(pieces, weight),
+        interpret=INTERPRET,
+        name="own_half",
+    )(first, pieces, weight)
+
+
+def last(first, pieces, weight, total, square):
+    rows = pieces.shape[1]
     seqs = rows // PROP
     cols = weight.shape[1]
     return pl.pallas_call(
         last_kernel,
         out_shape=jax.ShapeDtypeStruct((seqs, PROP, cols), jnp.bfloat16),
-        in_specs=[pl.BlockSpec(memory_space=pltpu.SMEM)] + vmem(3),
+        in_specs=[pl.BlockSpec(memory_space=pltpu.SMEM)] + vmem(4),
         out_specs=vmem(1)[0],
         scratch_shapes=[pltpu.VMEM((seqs, PROP, cols), jnp.float32)],
-        compiler_params=pltpu.CompilerParams(vmem_limit_bytes=20 << 20),
-        cost_estimate=pl.CostEstimate(
-            flops=2 * rows * HG * G * HD * cols, bytes_accessed=2 << 20, transcendentals=rows
-        ),
+        compiler_params=pltpu.CompilerParams(vmem_limit_bytes=16 << 20),
+        cost_estimate=cost_of(pieces, weight),
         interpret=INTERPRET,
         name="last",
-    )(group, own, other, weight)
+    )(first, pieces, weight, total, square)
 
 
 def prepared(
@@ -436,7 +476,7 @@
         jnp.transpose(surplus_fading, (1, 2, 3, 0)),
         hidden_carried_memory.reshape(seqs, heads * HD, N),
     )
-    return (wx, wz, wb, wc, in_vmem(narrow), in_hbm(wide), in_hbm(recent))
+    return (wx, in_hbm(wz), in_hbm(wb), wc, in_vmem(narrow), in_hbm(wide), in_hbm(recent))
 
 
 def shards(candidate_vectors, leading_scaling_factor, lane_feed_matrix, final_valve_matrix,
@@ -453,10 +493,12 @@
         shrink_speed_exponent, lane_bypass_factor, *memories,
     )
     gated = mixer(pieces, *rest)
-    along = lax.all_gather(gated, KV)
+    rings = [[G * z + (z + t) % G for z in range(lax.axis_size(KV))] for t in range(G)]
+    along = lax.all_gather(gated, (KV, "tp"), axis_index_groups=rings)
     swapped = lax.ppermute(along, "tp", [(0, 1), (1, 0)])
     weight = final_linear_matrix.reshape(HG * G * HD, -1)
-    return last(lax.axis_index("tp").reshape(1), along, swapped, weight)
+    first = ((lax.axis_index(KV) + lax.axis_index("tp")) % G).reshape(1)
+    return last(first, swapped, weight, *own_half(first, along, weight))
 
 
 def solution(mesh):

time: 108 us -> 104 us (0.963)
  starting transfers between devices: 53.6 us -> 46.4 us
  blocking collectives: 34.2 us -> 36.6 us
  waiting for transfers between devices: 5.99 us -> 8.11 us
  local copies, waits for them, and re-layouts: 5.67 us -> 4.39 us
    ppermute x1, starting transfers between devices: 9.22 us -> 2.06 us  [shards(): swapped = lax.ppermute(along, 'tp', [(0, 1), (1, 0)])]
    all_gather x1, blocking collectives: 25.3 us -> 29.2 us  [shards(): along = lax.all_gather(gated, (KV, 'tp'), axis_index_groups=rings)]
    all_to_all x1, waiting for transfers between devices: 4.48 us -> 6.68 us  [shards(): along = lax.all_to_all(copies, KV, split_axis=0, concat_axis=0, tiled=True)]
    all_gather x1, blocking collectives: 8.9 us -> 7.33 us  [shards(): pieces = lax.all_gather(along, 'tp')]
    unnamed x19 -> x15, local copies, waits for them, and re-layouts: 2.7 us -> 1.43 us
where the time goes in v4:
time: 104 us
  starting transfers between devices  46.4 us (45%)
  blocking collectives  36.6 us (35%)
  waiting for transfers between devices  8.11 us (8%)
  Pallas kernels  6.98 us (7%)
  local copies, waits for them, and re-layouts  4.39 us (4%)
  other arithmetic  1.28 us (1%)
    all_to_all x1, starting transfers between devices, shards(): along = lax.all_to_all(copies, KV, split_axis=0, concat_axis=0, tiled=True)  44.4 us
    all_gather x1, blocking collectives, shards(): along = lax.all_gather(gated, (KV, 'tp'), axis_index_groups=rings)  29.2 us
    all_gather x1, blocking collectives, shards(): pieces = lax.all_gather(along, 'tp')  7.33 us
    all_to_all x1, waiting for transfers between devices, shards(): along = lax.all_to_all(copies, KV, split_axis=0, concat_axis=0, tiled=True)  6.68 us
    pallas_call x1, Pallas kernels, mixer(): pl.pallas_call(mixer_kernel, out_shape=jax.ShapeDtypeStruct((2 * half, 2...  2.9 us
  transfers between devices with their start and end apart: 2, of which 2 were waited for; matrix products, arithmetic and copies ran while one was open for 5% of the time, Pallas kernels for 2%

profile of v4, /device:TPU:65, one launch (start us, length us, event | category | flops | bytes accessed | tf_op | source)
XLA Modules:
  0.0 103.9 jit_solution(326430827953407985)
XLA Ops:
  0.0 0.0 copy-start
  0.0 0.0 copy-start.6
  0.0 0.8 copy-done.6
  0.8 0.8 pack.1
  1.6 0.0 copy-start.2
  1.6 0.0 copy-start.3
  1.6 44.4 %all-to-all-start = ((bf16[16,64,128]{2,1,0:T(8,128)(2,1)}), bf16[16,64,128]{2,1,0:T(8,128)(2,1)S(1)}, u32[]{:S(2)}, u32[]{:S(2)}) async-start(bf16[16,64,128]{2,1,0:T(8,128)(2,1)} %pack.1), calls=%async_computation | async-start | bytes 524288 | tf_op jit(solution)/shard_map/all_to_all | solution.py:487
  46.0 1.3 %reshape.44.refs_0_ = bf16[1,2048]{1,0:T(2,128)(2,1)} reshape(bf16[2048]{0:T(1024)(128)(2,1)} %param.22) | data formatting | bytes 8192 | tf_op jit(solution)/shard_map/reshape | solution.py:465
  47.3 0.0 copy-done
  47.3 0.6 copy.33
  47.9 1.0 reshape.54
  49.0 0.6 copy.30.refs_2_
  49.6 1.3 %pad_maximum_fusion.refs_8_ = f32[3,2]{1,0:T(4,128)} fusion(f32[1,2]{1,0:T(1,128)} %bitcast.54, f32[1,2]{1,0:T(1,128)} %bitcast.55, f32[1,2]{1,0:T(1,128)} %bitcast.56), kind=kLoop, calls=%fused_computation.1 | loop fusion | flops 12 | bytes 48 | tf_op jit(solution)/shard_map/stack | solution.py:461
  50.9 2.0 %prep.1 = (f32[152,128]{1,0:T(8,128)S(1)}, bf16[35,128,128]{2,1,0:T(8,128)(2,1)S(1)}, bf16[416,128]{1,0:T(8,128)(2,1)S(1)}) custom-call(bf16[1,2048]{1,0:T(2,128)(2,1)} %reshape.44.refs_0_, bf16[2,2048]{1,0:T(2,128)(2,1)} %bitcast.50, bf16[7,32,128]{2,1,0:T(8,128)(2,1)} %copy.30.refs_2_, bf16[7,32,128]{2,1,0:T(8,128)(2,1)} %bitcast.48, ...), custom_call_target="tpu_custom_call" | custom-call | flops 16777216 | bytes 4194304 | tf_op jit(solution)/shard_map/prep/pallas_call | solution.py:348
  52.9 0.0 copy-start.4
  52.9 0.0 copy-start.5
  52.9 6.7 %all-to-all-done = bf16[16,64,128]{2,1,0:T(8,128)(2,1)S(1)} async-done(((bf16[16,64,128]{2,1,0:T(8,128)(2,1)}), bf16[16,64,128]{2,1,0:T(8,128)(2,1)S(1)}, u32[]{:S(2)}, u32[]{:S(2)}) %all-to-all-start) | async-done | bytes 262176 | tf_op jit(solution)/shard_map/all_to_all | solution.py:487
  59.6 7.3 %all-gather = bf16[32,64,128]{2,1,0:T(8,128)(2,1)S(1)} all-gather(bf16[16,64,128]{2,1,0:T(8,128)(2,1)S(1)} %all-to-all-done), channel_id=2, replica_groups=mesh['grp'=2,'dp'=8,'kv'=16,'tp'=2] {'tp'}, dimensions={0}, use_global_device_ids=true | all-gather | bytes 786432 | tf_op jit(solution)/shard_map/all_gather | solution.py:488
  66.9 0.0 copy-done.4
  66.9 0.0 copy-done.5
  66.9 0.0 copy-done.2
  66.9 0.0 copy-done.3
  66.9 0.0 copy-start.1
  66.9 2.9 %mixer.1 = bf16[128,128]{1,0:T(8,128)(2,1)S(1)} custom-call(bf16[2,16,64,128]{3,2,1,0:T(8,128)(2,1)S(1)} %bitcast.39, bf16[128,2048]{1,0:T(8,128)(2,1)S(1)} %bitcast.42, bf16[128,2048]{1,0:T(8,128)(2,1)} %bitcast.45, bf16[2048,128]{1,0:T(8,128)(2,1)} %bitcast.46, bf16[2048,128]{1,0:T(8,128)(2,1)S(1)} %bitcast.43, ...), custom_call_target="tpu_custom_call" | custom-call | flops 335544320 | bytes 5242880 | tf_op jit(solution)/shard_map/mixer/pallas_call | solution.py:368
  69.8 29.2 %all-gather.1 = bf16[2048,128]{1,0:T(8,128)(2,1)S(1)} all-gather(bf16[128,128]{1,0:T(8,128)(2,1)S(1)} %mixer.1), channel_id=3, replica_groups={{0,3,4,7,8,11,12,15,16,19,20,23,24,27,28,31},{1,2,5,6,9,10,13,14,17,18,..., dimensions={0}, use_global_device_ids=true | all-gather | bytes 557056 | tf_op jit(solution)/shard_map/all_gather | solution.py:497
  99.1 2.1 %collective-permute-start = (bf16[16,128,128]{2,1,0:T(8,128)(2,1)S(1)}, bf16[16,128,128]{2,1,0:T(8,128)(2,1)S(1)}, u32[]{:S(2)}, u32[]{:S(2)}) collective-permute-start(bf16[16,128,128]{2,1,0:T(8,128)(2,1)S(1)} %bitcast.40), channel_id=1, source_target_pairs={{0,1},{1,0},{2,3},{3,2},{4,5},{5,4},{6,7},{7,6},{8,9},{9,8},{10,11... | collective-permute-start | bytes 1572872 | tf_op jit(solution)/shard_map/ppermute | solution.py:498
  101.2 0.0 copy-done.1
  101.2 0.3 own_half.1
  101.5 1.4 %collective-permute-done.pieces_ref = bf16[16,128,128]{2,1,0:T(8,128)(2,1)S(1)} collective-permute-done((bf16[16,128,128]{2,1,0:T(8,128)(2,1)S(1)}, bf16[16,128,128]{2,1,0:T(8,128)(2,1)S(1)}, u32[]{:S(2)}, u32[]{:S(2)}) %collective-permute-start) | collective-permute-done | bytes 524320 | tf_op jit(solution)/shard_map/ppermute | solution.py:498
  102.9 1.0 last.1
  (1 shorter events, 0.0 us)
Async XLA Ops:
  0.0 47.3 %copy-start = (bf16[2048,32,2]{0,2,1:T(2,128)(2,1)S(1)}, bf16[2048,32,2]{0,2,1:T(2,128)(2,1)}, u32[]{:S(2)}) copy-start(bf16[2048,32,2]{0,2,1:T(2,128)(2,1)} %param.25) | copy-start | bytes 786436
  0.0 0.8 copy-start.6
  1.6 65.3 %copy-start.2 = (bf16[2048,2,1,64]{0,3,2,1:T(8,128)(2,1)S(1)}, bf16[2048,2,1,64]{0,3,2,1:T(8,128)(2,1)}, u32[]{:S(2)}) copy-start(bf16[2048,2,1,64]{0,3,2,1:T(8,128)(2,1)} %param.23) | copy-start | bytes 1572868
  1.6 65.3 %copy-start.3 = (bf16[2048,1,128]{2,0,1:T(8,128)(2,1)S(1)}, bf16[2048,1,128]{2,0,1:T(8,128)(2,1)}, u32[]{:S(2)}) copy-start(bf16[2048,1,128]{2,0,1:T(8,128)(2,1)} %param.27) | copy-start | bytes 1572868
  1.6 57.9 %all-to-all-start = ((bf16[16,64,128]{2,1,0:T(8,128)(2,1)}), bf16[16,64,128]{2,1,0:T(8,128)(2,1)S(1)}, u32[]{:S(2)}, u32[]{:S(2)}) async-start(bf16[16,64,128]{2,1,0:T(8,128)(2,1)} %pack.1), calls=%async_computation | async-start | bytes 524288 | tf_op jit(solution)/shard_map/all_to_all | solution.py:487
  52.9 14.0 %copy-start.4 = (bf16[416,128]{1,0:T(8,128)(2,1)}, bf16[416,128]{1,0:T(8,128)(2,1)S(1)}, u32[]{:S(2)}) copy-start(bf16[416,128]{1,0:T(8,128)(2,1)S(1)} %get-tuple-element.12.recent_far) | copy-start | bytes 319492
  52.9 14.0 %copy-start.5 = (f32[152,128]{1,0:T(8,128)}, f32[152,128]{1,0:T(8,128)S(1)}, u32[]{:S(2)}) copy-start(f32[152,128]{1,0:T(8,128)S(1)} %get-tuple-element.11.wide_far) | copy-start | bytes 233476
  66.9 34.2 %copy-start.1 = (bf16[32,2,64,64]{3,2,1,0:T(8,128)(2,1)S(1)}, bf16[32,2,64,64]{3,2,1,0:T(8,128)(2,1)}, u32[]{:S(2)}) copy-start(bf16[32,2,64,64]{3,2,1,0:T(8,128)(2,1)} %param.34) | copy-start | bytes 1572868
  99.1 3.8 %collective-permute-start = (bf16[16,128,128]{2,1,0:T(8,128)(2,1)S(1)}, bf16[16,128,128]{2,1,0:T(8,128)(2,1)S(1)}, u32[]{:S(2)}, u32[]{:S(2)}) collective-permute-start(bf16[16,128,128]{2,1,0:T(8,128)(2,1)S(1)} %bitcast.40), channel_id=1, source_target_pairs={{0,1},{1,0},{2,3},{3,2},{4,5},{5,4},{6,7},{7,6},{8,9},{9,8},{10,11... | collective-permute-start | bytes 1572872 | tf_op jit(solution)/shard_map/ppermute | solution.py:498

commit v5 on v4

--- a/solution.py
+++ b/solution.py
@@ -55,8 +55,11 @@
 
 def places(seqs):
     at, row = {}, 0
-    sizes = (("taps", 16), ("heads", 8), ("fading", PROP * seqs), ("end", 0))
-    for name, size in sizes:
+    sizes = (("state", seqs * N), ("dt", 16 * (D // N)), ("recent", 3 * (CONV - 1) * seqs))
+    sizes += (("parent", PROP * seqs), ("gain", D // N))
+    for part in range(3):
+        sizes += ((f"taps{part}", 16), (f"heads{part}", 16), (f"fading{part}", PROP * seqs))
+    for name, size in (*sizes, ("end", 0)):
         at[name] = row
         row += size
     return at
@@ -64,8 +67,7 @@
 
 def prep_kernel(*refs):
     count = 13
-    sources, held, sems = refs[:count], refs[count + 3 : -1], refs[-1]
-    wide_out, narrow_out, recent_out = refs[count : count + 3]
+    sources, all_out, held, sems = refs[:count], refs[count], refs[count + 1 : -1], refs[-1]
     copies = [pltpu.make_async_copy(sources[k], held[k], sems.at[k]) for k in range(count)]
     for copy in copies:
         copy.start()
@@ -91,28 +93,34 @@
         copy.wait()
     def put(name, index, value):
         start = at[name] + index * value.shape[0]
-        wide_out[start : start + value.shape[0], :] = value
+        all_out[start : start + value.shape[0], :] = value.astype(jnp.bfloat16)
+
+    def put_parts(name, index, value):
+        for part in range(3):
+            put(f"{name}{part}", index, value)
+            value = value - value.astype(jnp.bfloat16).astype(f32)
+
+    def rows_of(lines):
+        return jnp.concatenate(lines + [jnp.zeros((16 - len(lines), N), f32)], axis=0)
 
     for k in range(D // N):
         pair = [
             jnp.broadcast_to(dt_ref[h : h + 1, k * N : (k + 1) * N].astype(f32), (8, N))
             for h in range(2)
         ]
-        row = (k % 8) * 16
-        narrow_out[seqs + k // 8, row : row + 16, :] = jnp.concatenate(pair, axis=0).astype(
-            jnp.bfloat16
-        )
+        put("dt", k, jnp.concatenate(pair, axis=0))
     gains = [gain_ref[:, k * N : (k + 1) * N].astype(f32) for k in range(D // N)]
-    narrow_out[seqs + D // N // 8, : D // N, :] = jnp.concatenate(gains, axis=0).astype(jnp.bfloat16)
-    for t in range(CONV):
-        put("taps", t, jnp.concatenate([taps_x_ref[t, h] for h in range(2)], axis=1))
-        put("taps", CONV + t, taps_b_ref[t])
-        put("taps", 2 * CONV + t, taps_c_ref[t])
+    put("gain", 0, jnp.concatenate(gains, axis=0))
+    taps = [jnp.concatenate([taps_x_ref[t, h] for h in range(2)], axis=1) for t in range(CONV)]
+    taps += [taps_b_ref[t] for t in range(CONV)] + [taps_c_ref[t] for t in range(CONV)]
+    put_parts("taps", 0, rows_of(taps))
     one = lax.broadcasted_iota(jnp.int32, (1, 2 * HD), 1) < HD
     heads = heads_ref[...]
-    for place in range(3):
-        row = jnp.where(one, heads[place : place + 1, 0:1], heads[place : place + 1, 1:2])
-        put("heads", place, -jnp.exp(row) if place == 1 else row)
+    lines = [
+        jnp.where(one, heads[place : place + 1, 0:1], heads[place : place + 1, 1:2])
+        for place in range(3)
+    ]
+    put_parts("heads", 0, rows_of([lines[0], -jnp.exp(lines[1]), lines[2]]))
 
     def turned(lines):
         total = sum(line.shape[0] for line in lines)
@@ -128,23 +136,21 @@
     table = turned([parents_ref[...].astype(f32), admitted_ref[...].astype(f32)])
     admitted = wide(table[:, PROP : PROP + 1])
     for j in range(PROP):
-        start = 3 * (CONV - 1) + j
-        recent_out[start * seqs : (start + 1) * seqs, :] = wide(table[:, j : j + 1]).astype(jnp.bfloat16)
+        put("parent", j, wide(table[:, j : j + 1]))
     for which, mem_ref in enumerate((mem_x_ref, mem_b_ref, mem_c_ref)):
         for back in range(CONV - 1):
             offset = CONV - 2 - back
             value = mem_ref[offset].astype(f32)
             for step in range(1, PREV + 1):
                 value = jnp.where(admitted == step, mem_ref[offset + step].astype(f32), value)
-            start = which * (CONV - 1) + back
-            recent_out[start * seqs : (start + 1) * seqs, :] = value.astype(jnp.bfloat16)
+            put("recent", which * (CONV - 1) + back, value)
     fading = turned([fading_ref[j, h] for j in range(PROP) for h in range(2)])
     first_head = lax.broadcasted_iota(jnp.int32, (seqs, 2 * HD), 1) < HD
     for j in range(PROP):
         pair = [wide(fading[:, 2 * j + h : 2 * j + h + 1]) for h in range(2)]
-        put("fading", j, jnp.where(first_head, *pair))
+        put_parts("fading", j, jnp.where(first_head, *pair))
     copies[-1].wait()
-    narrow_out[:seqs] = state_ref[...].astype(jnp.bfloat16)
+    all_out[: seqs * N, :] = state_ref[...].reshape(seqs * N, N).astype(jnp.bfloat16)
 
 
 def mixer_kernel(
@@ -152,17 +158,14 @@
     wx_ref,
     wz_far,
     wb_far,
-    wc_ref,
-    narrow_ref,
-    wide_far,
-    recent_far,
+    wc_far,
+    tables_ref,
     out_ref,
     cc_all,
     read_all,
-    wide_ref,
-    recent_ref,
+    wc_ref,
+    wb_ref,
     wz_ref,
-    wb_ref,
     sems,
 ):
     half = pieces_ref.shape[2]
@@ -170,21 +173,25 @@
     rows = 2 * half
     kv_count = pieces_ref.shape[1]
     f32 = jnp.float32
-    copies = [
-        pltpu.make_async_copy(wide_far, wide_ref, sems.at[0]),
-        pltpu.make_async_copy(recent_far, recent_ref, sems.at[1]),
-        pltpu.make_async_copy(wb_far, wb_ref, sems.at[2]),
-        pltpu.make_async_copy(wz_far, wz_ref, sems.at[3]),
-    ]
-    for copy in copies:
-        copy.start()
+    wc_copy = pltpu.make_async_copy(wc_far, wc_ref, sems.at[0])
+    wb_copy = pltpu.make_async_copy(wb_far, wb_ref, sems.at[1])
+    wz_copy = pltpu.make_async_copy(wz_far, wz_ref, sems.at[2])
+    wc_copy.start()
+    wb_copy.start()
+    wz_copy.start()
     left = lax.broadcasted_iota(jnp.int32, (half, 2 * HD), 1) < HD
     at = places(seqs)
 
     def table(name, index, size):
-        return wide_ref[at[name] + index * size : at[name] + (index + 1) * size, :]
-
-    gains = narrow_ref[seqs + D // N // 8, : D // N, :].astype(f32)
+        return tables_ref[at[name] + index * size : at[name] + (index + 1) * size, :].astype(f32)
+
+    def whole(name, index, size):
+        high, middle, low = (table(f"{name}{part}", index, size) for part in range(3))
+        return high + middle + low
+
+    gains = table("gain", 0, D // N)
+    taps = whole("taps", 0, 16)
+    heads = whole("heads", 0, 16)
     scaled = []
     square = jnp.zeros((rows, 2 * HD), f32)
     for k in range(kv_count):
@@ -204,24 +211,16 @@
 
     across = (((1,), (1,)), ((), ()))
     down = (((1,), (0,)), ((), ()))
-    c_rows = times(wc_ref[...], down).astype(jnp.bfloat16).astype(f32)
     x_rows = times(wx_ref[...], across).astype(jnp.bfloat16).astype(f32)
-    chunks = [narrow_ref[seqs + k // 8, (k % 8) * 16 : (k % 8) * 16 + 16, :] for k in range(D // N)]
+    chunks = [tables_ref[at["dt"] + 16 * k : at["dt"] + 16 * (k + 1), :] for k in range(D // N)]
     dt_cols = times(jnp.concatenate(chunks, axis=1), across)
     dt_raw = jnp.where(
         lax.broadcasted_iota(jnp.int32, (rows, 2 * HD), 1) < HD,
         *(jnp.broadcast_to(dt_cols[:, c : c + 1], (rows, 2 * HD)) for c in (0, 8)),
     )
 
-    for copy in copies:
-        copy.wait()
-    b_rows = times(wb_ref[...], down).astype(jnp.bfloat16).astype(f32)
-    z_rows = times(wz_ref[...], across).astype(jnp.bfloat16).astype(f32)
-
-    def recent(index):
-        return recent_ref[index * seqs : (index + 1) * seqs, :].astype(f32)
-
-    parent = [recent(3 * (CONV - 1) + j) for j in range(PROP)]
+
+    parent = [table("parent", j, seqs) for j in range(PROP)]
     child = [[parent[j] == i for i in range(j)] for j in range(PROP)]
 
     def block(array, j):
@@ -230,7 +229,7 @@
     def conv(row_array, which):
         history = []
         outs = []
-        roots = [recent(which * (CONV - 1) + back) for back in range(CONV - 1)]
+        roots = [table("recent", which * (CONV - 1) + back, seqs) for back in range(CONV - 1)]
         for j in range(PROP):
             inputs = [block(row_array, j)]
             for back in range(CONV - 1):
@@ -241,30 +240,22 @@
             history.append(inputs)
             total = None
             for lag in range(CONV):
-                term = table("taps", which * CONV + CONV - 1 - lag, 1) * inputs[lag]
+                place = which * CONV + CONV - 1 - lag
+                term = taps[place : place + 1, :] * inputs[lag]
                 total = term if total is None else total + term
             outs.append(jax.nn.silu(total))
         return outs
 
-    cc = conv(c_rows, 2)
-    for j in range(PROP):
-        cc_all[:, j, :] = cc[j]
-        cc_all[:, PROP + j, :] = cc[j]
-    for s in range(seqs):
-        read_all[s] = lax.dot_general(
-            cc_all[s].astype(jnp.bfloat16), narrow_ref[s], across, preferred_element_type=f32
-        )
     xc = conv(x_rows, 0)
-    bc = conv(b_rows, 1)
-
-    offset, speed, bypass = (table("heads", place, 1) for place in range(3))
+
+    offset, speed, bypass = (heads[place : place + 1, :] for place in range(3))
     level = []
     moved = []
     above = []
     for j in range(PROP):
         raw = block(dt_raw, j) + offset
         step = jnp.maximum(raw, 0.0) + jnp.log1p(jnp.exp(-jnp.abs(raw)))
-        own = speed * step + table("fading", j, seqs)
+        own = speed * step + whole("fading", j, seqs)
         prior = jnp.zeros_like(own)
         for i in range(j):
             prior = jnp.where(child[j][i], level[i], prior)
@@ -277,8 +268,25 @@
                 reach = reach | (child[j][p] & above[p][i])
             line.append(reach)
         above.append(line)
-    for j in range(PROP):
-        y = jnp.exp(level[j]) * read_all[:, j, :] + bypass * xc[j]
+    wc_copy.wait()
+    c_rows = times(wc_ref[...], down).astype(jnp.bfloat16).astype(f32)
+    cc = conv(c_rows, 2)
+    for j in range(PROP):
+        cc_all[:, j, :] = cc[j]
+        cc_all[:, PROP + j, :] = cc[j]
+    for s in range(seqs):
+        read_all[s] = lax.dot_general(
+            cc_all[s].astype(jnp.bfloat16),
+            tables_ref[s * N : (s + 1) * N, :],
+            across,
+            preferred_element_type=f32,
+        )
+    wb_copy.wait()
+    b_rows = times(wb_ref[...], down).astype(jnp.bfloat16).astype(f32)
+    bc = conv(b_rows, 1)
+    inner = []
+    for j in range(PROP):
+        y = bypass * xc[j]
         for i in range(j + 1):
             score = jnp.sum(cc[j] * bc[i], axis=1, keepdims=True)
             if i == j:
@@ -286,8 +294,13 @@
             else:
                 fall = jnp.exp(jnp.minimum(level[j] - level[i], 0.0))
                 y = y + jnp.where(above[j][i], fall * (score * moved[i]), 0.0)
-        gated = (y * jax.nn.silu(block(z_rows, j))).astype(jnp.bfloat16)
-        out_ref[j * seqs : (j + 1) * seqs, :] = gated
+        inner.append(y)
+    outs = [jnp.exp(level[j]) * read_all[:, j, :] + inner[j] for j in range(PROP)]
+    wz_copy.wait()
+    z_rows = times(wz_ref[...], across).astype(jnp.bfloat16).astype(f32)
+    for j in range(PROP):
+        gated = outs[j] * jax.nn.silu(block(z_rows, j))
+        out_ref[j * seqs : (j + 1) * seqs, :] = gated.astype(jnp.bfloat16)
 
 
 def share_of(pieces_ref, first, weight_ref):
@@ -347,13 +360,9 @@
     seqs = state.shape[0]
     return pl.pallas_call(
         prep_kernel,
-        out_shape=[
-            jax.ShapeDtypeStruct((places(seqs)["end"], N), jnp.float32),
-            pltpu.VMEM((seqs + D // N // 8 + 1, N, N), jnp.bfloat16),
-            jax.ShapeDtypeStruct(((3 * (CONV - 1) + PROP) * seqs, N), jnp.bfloat16),
-        ],
+        out_shape=pltpu.VMEM((places(seqs)["end"], N), jnp.bfloat16),
         in_specs=[pl.BlockSpec(memory_space=pltpu.HBM)] * len(inputs),
-        out_specs=vmem(3),
+        out_specs=vmem(1)[0],
         scratch_shapes=[pltpu.VMEM(x.shape, x.dtype) for x in inputs]
         + [pltpu.SemaphoreType.DMA((len(inputs),))],
         compiler_params=pltpu.CompilerParams(vmem_limit_bytes=16 << 20),
@@ -368,13 +377,13 @@
     return pl.pallas_call(
         mixer_kernel,
         out_shape=jax.ShapeDtypeStruct((2 * half, 2 * HD), jnp.bfloat16),
-        in_specs=vmem(2) + hbm(2) + vmem(2) + hbm(2),
+        in_specs=vmem(2) + hbm(3) + vmem(1),
         out_specs=vmem(1)[0],
         scratch_shapes=[
             pltpu.VMEM((half // 2, 2 * PROP, N), jnp.float32),
             pltpu.VMEM((half // 2, 2 * PROP, 2 * HD), jnp.float32),
-            *(pltpu.VMEM(x.shape, x.dtype) for x in (rest[-2], rest[-1], rest[1], rest[2])),
-            pltpu.SemaphoreType.DMA((4,)),
+            *(pltpu.VMEM(x.shape, x.dtype) for x in (rest[3], rest[2], rest[1])),
+            pltpu.SemaphoreType.DMA((3,)),
         ],
         compiler_params=pltpu.CompilerParams(vmem_limit_bytes=20 << 20),
         cost_estimate=pl.CostEstimate(
@@ -461,7 +470,7 @@
     head_rows = jnp.stack(
         [x.reshape(heads) for x in (increment_offset, shrink_speed_exponent, lane_bypass_factor)]
     )
-    wide, narrow, recent = prep(
+    tables = prep(
         leading_scaling_factor.reshape(1, D),
         dt_own.reshape(heads, D),
         jnp.transpose(lane_filter_memory, (1, 0, 2, 3, 4)).reshape(WIN, seqs, heads * HD),
@@ -476,7 +485,7 @@
         jnp.transpose(surplus_fading, (1, 2, 3, 0)),
         hidden_carried_memory.reshape(seqs, heads * HD, N),
     )
-    return (wx, in_hbm(wz), in_hbm(wb), wc, in_vmem(narrow), in_hbm(wide), in_hbm(recent))
+    return (wx, in_hbm(wz), in_hbm(wb), in_hbm(wc), in_vmem(tables))
 
 
 def shards(candidate_vectors, leading_scaling_factor, lane_feed_matrix, final_valve_matrix,

time: 104 us -> 104 us (level)
  no operation moved by 1% of the time
where the time goes in v5:
time: 104 us
  starting transfers between devices  46.3 us (45%)
  blocking collectives  36.5 us (35%)
  waiting for transfers between devices  8.04 us (8%)
  Pallas kernels  7.09 us (7%)
  local copies, waits for them, and re-layouts  4.38 us (4%)
  other arithmetic  1.29 us (1%)
    all_to_all x1, starting transfers between devices, shards(): along = lax.all_to_all(copies, KV, split_axis=0, concat_axis=0, tiled=True)  44.2 us
    all_gather x1, blocking collectives, shards(): along = lax.all_gather(gated, (KV, 'tp'), axis_index_groups=rings)  29.2 us
    all_gather x1, blocking collectives, shards(): pieces = lax.all_gather(along, 'tp')  7.33 us
    all_to_all x1, waiting for transfers between devices, shards(): along = lax.all_to_all(copies, KV, split_axis=0, concat_axis=0, tiled=True)  6.63 us
    pallas_call x1, Pallas kernels, mixer(): pl.pallas_call(mixer_kernel, out_shape=jax.ShapeDtypeStruct((2 * half, 2...  2.98 us
    ppermute x1, starting transfers between devices, shards(): swapped = lax.ppermute(along, 'tp', [(0, 1), (1, 0)])  2.08 us
  transfers between devices with their start and end apart: 2, of which 2 were waited for; matrix products, arithmetic and copies ran while one was open for 5% of the time, Pallas kernels for 2%

profile of v5, /device:TPU:65, one launch (start us, length us, event | category | flops | bytes accessed | tf_op | source)
XLA Modules:
  0.0 103.7 jit_solution(9113206943440714508)
XLA Ops:
  0.0 0.0 copy-start
  0.0 0.0 copy-start.3
  0.0 0.8 copy-done.3
  0.8 0.8 pack.1
  1.6 44.2 %all-to-all-start = ((bf16[16,64,128]{2,1,0:T(8,128)(2,1)}), bf16[16,64,128]{2,1,0:T(8,128)(2,1)S(1)}, u32[]{:S(2)}, u32[]{:S(2)}) async-start(bf16[16,64,128]{2,1,0:T(8,128)(2,1)} %pack.1), calls=%async_computation | async-start | bytes 524288 | tf_op jit(solution)/shard_map/all_to_all | solution.py:496
  45.9 1.3 %reshape.44.refs_0_ = bf16[1,2048]{1,0:T(2,128)(2,1)} reshape(bf16[2048]{0:T(1024)(128)(2,1)} %param.22) | data formatting | bytes 8192 | tf_op jit(solution)/shard_map/reshape | solution.py:474
  47.2 0.0 copy-done
  47.2 0.6 copy.33
  47.8 1.0 reshape.54
  48.8 0.6 copy.30.refs_2_
  49.4 1.3 %pad_maximum_fusion.refs_8_ = f32[3,2]{1,0:T(4,128)} fusion(f32[1,2]{1,0:T(1,128)} %bitcast.54, f32[1,2]{1,0:T(1,128)} %bitcast.55, f32[1,2]{1,0:T(1,128)} %bitcast.56), kind=kLoop, calls=%fused_computation.1 | loop fusion | flops 12 | bytes 48 | tf_op jit(solution)/shard_map/stack | solution.py:470
  50.7 0.0 copy-start.2
  50.7 2.1 %prep.1.tables_ref = bf16[5264,128]{1,0:T(8,128)(2,1)S(1)} custom-call(bf16[1,2048]{1,0:T(2,128)(2,1)} %reshape.44.refs_0_, bf16[2,2048]{1,0:T(2,128)(2,1)} %bitcast.50, bf16[7,32,128]{2,1,0:T(8,128)(2,1)} %copy.30.refs_2_, bf16[7,32,128]{2,1,0:T(8,128)(2,1)} %bitcast.48, bf16[7,32,128]{2,1,0:T(8,128)(2,1)} %bitcast.49, f32[4,2,1,64]{3,2,1,0:T(1,128)} %refs_5_.1, ...), custom_call_target="tpu_custom_call" | custom-call | flops 16777216 | bytes 4194304 | tf_op jit(solution)/shard_map/prep/pallas_call | solution.py:361
  52.8 6.6 %all-to-all-done = bf16[16,64,128]{2,1,0:T(8,128)(2,1)S(1)} async-done(((bf16[16,64,128]{2,1,0:T(8,128)(2,1)}), bf16[16,64,128]{2,1,0:T(8,128)(2,1)S(1)}, u32[]{:S(2)}, u32[]{:S(2)}) %all-to-all-start) | async-done | bytes 262176 | tf_op jit(solution)/shard_map/all_to_all | solution.py:496
  59.4 7.3 %all-gather = bf16[32,64,128]{2,1,0:T(8,128)(2,1)S(1)} all-gather(bf16[16,64,128]{2,1,0:T(8,128)(2,1)S(1)} %all-to-all-done), channel_id=2, replica_groups=mesh['grp'=2,'dp'=8,'kv'=16,'tp'=2] {'tp'}, dimensions={0}, use_global_device_ids=true | all-gather | bytes 786432 | tf_op jit(solution)/shard_map/all_gather | solution.py:497
  66.8 0.0 copy-done.2
  66.8 0.0 copy-start.1
  66.8 3.0 %mixer.1 = bf16[128,128]{1,0:T(8,128)(2,1)S(1)} custom-call(bf16[2,16,64,128]{3,2,1,0:T(8,128)(2,1)S(1)} %bitcast.39, bf16[128,2048]{1,0:T(8,128)(2,1)S(1)} %bitcast.42, bf16[128,2048]{1,0:T(8,128)(2,1)} %bitcast.44, bf16[2048,128]{1,0:T(8,128)(2,1)} %bitcast.45, bf16[2048,128]{1,0:T(8,128)(2,1)} %bitcast.46, bf16[5264,128]{1,0:T(8,128)(2,1)S(1)} %prep.1.tables_ref), custom_call_target="tpu_custom_call" | custom-call | flops 335544320 | bytes 5242880 | tf_op jit(solution)/shard_map/mixer/pallas_call | solution.py:377
  69.7 29.2 %all-gather.1 = bf16[2048,128]{1,0:T(8,128)(2,1)S(1)} all-gather(bf16[128,128]{1,0:T(8,128)(2,1)S(1)} %mixer.1), channel_id=3, replica_groups={{0,3,4,7,8,11,12,15,16,19,20,23,24,27,28,31},{1,2,5,6,9,10,13,14,17,18,..., dimensions={0}, use_global_device_ids=true | all-gather | bytes 557056 | tf_op jit(solution)/shard_map/all_gather | solution.py:506
  98.9 2.1 %collective-permute-start = (bf16[16,128,128]{2,1,0:T(8,128)(2,1)S(1)}, bf16[16,128,128]{2,1,0:T(8,128)(2,1)S(1)}, u32[]{:S(2)}, u32[]{:S(2)}) collective-permute-start(bf16[16,128,128]{2,1,0:T(8,128)(2,1)S(1)} %bitcast.40), channel_id=1, source_target_pairs={{0,1},{1,0},{2,3},{3,2},{4,5},{5,4},{6,7},{7,6},{8,9},{9,8},{10,11... | collective-permute-start | bytes 1572872 | tf_op jit(solution)/shard_map/ppermute | solution.py:507
  101.0 0.0 copy-done.1
  101.0 0.3 own_half.1
  101.3 1.4 %collective-permute-done.pieces_ref = bf16[16,128,128]{2,1,0:T(8,128)(2,1)S(1)} collective-permute-done((bf16[16,128,128]{2,1,0:T(8,128)(2,1)S(1)}, bf16[16,128,128]{2,1,0:T(8,128)(2,1)S(1)}, u32[]{:S(2)}, u32[]{:S(2)}) %collective-permute-start) | collective-permute-done | bytes 524320 | tf_op jit(solution)/shard_map/ppermute | solution.py:507
  102.8 0.9 last.1
  (1 shorter events, 0.0 us)
Async XLA Ops:
  0.0 47.2 %copy-start = (bf16[2048,32,2]{0,2,1:T(2,128)(2,1)S(1)}, bf16[2048,32,2]{0,2,1:T(2,128)(2,1)}, u32[]{:S(2)}) copy-start(bf16[2048,32,2]{0,2,1:T(2,128)(2,1)} %param.25) | copy-start | bytes 786436
  0.0 0.8 copy-start.3
  1.6 57.8 %all-to-all-start = ((bf16[16,64,128]{2,1,0:T(8,128)(2,1)}), bf16[16,64,128]{2,1,0:T(8,128)(2,1)S(1)}, u32[]{:S(2)}, u32[]{:S(2)}) async-start(bf16[16,64,128]{2,1,0:T(8,128)(2,1)} %pack.1), calls=%async_computation | async-start | bytes 524288 | tf_op jit(solution)/shard_map/all_to_all | solution.py:496
  50.7 16.0 %copy-start.2 = (bf16[2048,2,1,64]{0,3,2,1:T(8,128)(2,1)S(1)}, bf16[2048,2,1,64]{0,3,2,1:T(8,128)(2,1)}, u32[]{:S(2)}) copy-start(bf16[2048,2,1,64]{0,3,2,1:T(8,128)(2,1)} %param.23) | copy-start | bytes 1572868
  66.8 34.3 %copy-start.1 = (bf16[32,2,64,64]{3,2,1,0:T(8,128)(2,1)S(1)}, bf16[32,2,64,64]{3,2,1,0:T(8,128)(2,1)}, u32[]{:S(2)}) copy-start(bf16[32,2,64,64]{3,2,1,0:T(8,128)(2,1)} %param.34) | copy-start | bytes 1572868
  98.9 3.8 %collective-permute-start = (bf16[16,128,128]{2,1,0:T(8,128)(2,1)S(1)}, bf16[16,128,128]{2,1,0:T(8,128)(2,1)S(1)}, u32[]{:S(2)}, u32[]{:S(2)}) collective-permute-start(bf16[16,128,128]{2,1,0:T(8,128)(2,1)S(1)} %bitcast.40), channel_id=1, source_target_pairs={{0,1},{1,0},{2,3},{3,2},{4,5},{5,4},{6,7},{7,6},{8,9},{9,8},{10,11... | collective-permute-start | bytes 1572872 | tf_op jit(solution)/shard_map/ppermute | solution.py:507

commit v6 on v5

--- a/solution.py
+++ b/solution.py
@@ -326,7 +326,10 @@
     return total, square
 
 
-def own_kernel(first_ref, pieces_ref, weight_ref, total_ref, square_ref):
+def own_kernel(first_ref, pieces_ref, weight_far, total_ref, square_ref, weight_ref, sem):
+    copy = pltpu.make_async_copy(weight_far, weight_ref, sem)
+    copy.start()
+    copy.wait()
     total_ref[...], square_ref[...] = share_of(pieces_ref, first_ref[0], weight_ref)
 
 
@@ -408,14 +411,16 @@
         out_shape=[
             jax.ShapeDtypeStruct((rows, weight.shape[1]), jnp.float32),
             jax.ShapeDtypeStruct((rows, 2 * HD), jnp.float32),
+            pltpu.VMEM(weight.shape, weight.dtype),
         ],
-        in_specs=[pl.BlockSpec(memory_space=pltpu.SMEM)] + vmem(2),
-        out_specs=vmem(2),
+        in_specs=[pl.BlockSpec(memory_space=pltpu.SMEM)] + vmem(1) + hbm(1),
+        out_specs=vmem(3),
+        scratch_shapes=[pltpu.SemaphoreType.DMA],
         compiler_params=pltpu.CompilerParams(vmem_limit_bytes=16 << 20),
         cost_estimate=cost_of(pieces, weight),
         interpret=INTERPRET,
         name="own_half",
-    )(first, pieces, weight)
+    )(first, pieces, in_hbm(weight))
 
 
 def last(first, pieces, weight, total, square):
@@ -507,7 +512,8 @@
     swapped = lax.ppermute(along, "tp", [(0, 1), (1, 0)])
     weight = final_linear_matrix.reshape(HG * G * HD, -1)
     first = ((lax.axis_index(KV) + lax.axis_index("tp")) % G).reshape(1)
-    return last(first, swapped, weight, *own_half(first, along, weight))
+    total, square, held = own_half(first, along, weight)
+    return last(first, swapped, in_vmem(held), total, square)
 
 
 def solution(mesh):

time: 104 us -> 104 us (level)
  waiting for transfers between devices: 8.04 us -> 6.81 us
  Pallas kernels: 7.09 us -> 8.25 us
    pallas_call x1, Pallas kernels: 0.3 us -> 1.54 us  [own_half(): pl.pallas_call(own_kernel, out_shape=[jax.ShapeDtypeStruct((rows, weight....]
    ppermute x1, waiting for transfers between devices: 1.41 us -> 0.18 us  [shards(): swapped = lax.ppermute(along, 'tp', [(0, 1), (1, 0)])]
  transfers between devices with their start and end apart: 2 -> 2, of which waited for: 2 -> 2; matrix products, arithmetic and copies ran while one was open for 5% -> 5% of each run, Pallas kernels for 2% -> 3%
where the time goes in v6:
time: 104 us
  starting transfers between devices  46.3 us (45%)
  blocking collectives  36.5 us (35%)
  Pallas kernels  8.25 us (8%)
  waiting for transfers between devices  6.81 us (7%)
  local copies, waits for them, and re-layouts  4.38 us (4%)
  other arithmetic  1.28 us (1%)
    all_to_all x1, starting transfers between devices, shards(): along = lax.all_to_all(copies, KV, split_axis=0, concat_axis=0, tiled=True)  44.2 us
    all_gather x1, blocking collectives, shards(): along = lax.all_gather(gated, (KV, 'tp'), axis_index_groups=rings)  29.2 us
    all_gather x1, blocking collectives, shards(): pieces = lax.all_gather(along, 'tp')  7.33 us
    all_to_all x1, waiting for transfers between devices, shards(): along = lax.all_to_all(copies, KV, split_axis=0, concat_axis=0, tiled=True)  6.64 us
    pallas_call x1, Pallas kernels, mixer(): pl.pallas_call(mixer_kernel, out_shape=jax.ShapeDtypeStruct((2 * half, 2...  2.89 us
    ppermute x1, starting transfers between devices, shards(): swapped = lax.ppermute(along, 'tp', [(0, 1), (1, 0)])  2.08 us
  transfers between devices with their start and end apart: 2, of which 2 were waited for; matrix products, arithmetic and copies ran while one was open for 5% of the time, Pallas kernels for 3%

profile of v6, /device:TPU:65, one launch (start us, length us, event | category | flops | bytes accessed | tf_op | source)
XLA Modules:
  0.0 103.6 jit_solution(4830492059453812741)
XLA Ops:
  0.0 0.0 copy-start
  0.0 0.0 copy-start.2
  0.0 0.8 copy-done.2
  0.8 0.8 pack.1
  1.6 44.2 %all-to-all-start = ((bf16[16,64,128]{2,1,0:T(8,128)(2,1)}), bf16[16,64,128]{2,1,0:T(8,128)(2,1)S(1)}, u32[]{:S(2)}, u32[]{:S(2)}) async-start(bf16[16,64,128]{2,1,0:T(8,128)(2,1)} %pack.1), calls=%async_computation | async-start | bytes 524288 | tf_op jit(solution)/shard_map/all_to_all | solution.py:501
  45.9 1.3 %reshape.44.refs_0_ = bf16[1,2048]{1,0:T(2,128)(2,1)} reshape(bf16[2048]{0:T(1024)(128)(2,1)} %param.22) | data formatting | bytes 8192 | tf_op jit(solution)/shard_map/reshape | solution.py:479
  47.2 0.0 copy-done
  47.2 0.6 copy.33
  47.8 1.0 reshape.54
  48.8 0.6 copy.30.refs_2_
  49.4 1.3 %pad_maximum_fusion.refs_8_ = f32[3,2]{1,0:T(4,128)} fusion(f32[1,2]{1,0:T(1,128)} %bitcast.53, f32[1,2]{1,0:T(1,128)} %bitcast.54, f32[1,2]{1,0:T(1,128)} %bitcast.55), kind=kLoop, calls=%fused_computation.1 | loop fusion | flops 12 | bytes 48 | tf_op jit(solution)/shard_map/stack | solution.py:475
  50.7 0.0 copy-start.1
  50.7 2.1 %prep.1.tables_ref = bf16[5264,128]{1,0:T(8,128)(2,1)S(1)} custom-call(bf16[1,2048]{1,0:T(2,128)(2,1)} %reshape.44.refs_0_, bf16[2,2048]{1,0:T(2,128)(2,1)} %bitcast.49, bf16[7,32,128]{2,1,0:T(8,128)(2,1)} %copy.30.refs_2_, bf16[7,32,128]{2,1,0:T(8,128)(2,1)} %bitcast.47, bf16[7,32,128]{2,1,0:T(8,128)(2,1)} %bitcast.48, f32[4,2,1,64]{3,2,1,0:T(1,128)} %refs_5_.1, ...), custom_call_target="tpu_custom_call" | custom-call | flops 16777216 | bytes 4194304 | tf_op jit(solution)/shard_map/prep/pallas_call | solution.py:364
  52.8 6.6 %all-to-all-done = bf16[16,64,128]{2,1,0:T(8,128)(2,1)S(1)} async-done(((bf16[16,64,128]{2,1,0:T(8,128)(2,1)}), bf16[16,64,128]{2,1,0:T(8,128)(2,1)S(1)}, u32[]{:S(2)}, u32[]{:S(2)}) %all-to-all-start) | async-done | bytes 262176 | tf_op jit(solution)/shard_map/all_to_all | solution.py:501
  59.4 7.3 %all-gather = bf16[32,64,128]{2,1,0:T(8,128)(2,1)S(1)} all-gather(bf16[16,64,128]{2,1,0:T(8,128)(2,1)S(1)} %all-to-all-done), channel_id=2, replica_groups=mesh['grp'=2,'dp'=8,'kv'=16,'tp'=2] {'tp'}, dimensions={0}, use_global_device_ids=true | all-gather | bytes 786432 | tf_op jit(solution)/shard_map/all_gather | solution.py:502
  66.8 0.0 copy-done.1
  66.8 2.9 %mixer.1 = bf16[128,128]{1,0:T(8,128)(2,1)S(1)} custom-call(bf16[2,16,64,128]{3,2,1,0:T(8,128)(2,1)S(1)} %bitcast.37, bf16[128,2048]{1,0:T(8,128)(2,1)S(1)} %bitcast.40, bf16[128,2048]{1,0:T(8,128)(2,1)} %bitcast.43, bf16[2048,128]{1,0:T(8,128)(2,1)} %bitcast.44, bf16[2048,128]{1,0:T(8,128)(2,1)} %bitcast.45, bf16[5264,128]{1,0:T(8,128)(2,1)S(1)} %prep.1.tables_ref), custom_call_target="tpu_custom_call" | custom-call | flops 335544320 | bytes 5242880 | tf_op jit(solution)/shard_map/mixer/pallas_call | solution.py:380
  69.7 29.2 %all-gather.1 = bf16[2048,128]{1,0:T(8,128)(2,1)S(1)} all-gather(bf16[128,128]{1,0:T(8,128)(2,1)S(1)} %mixer.1), channel_id=3, replica_groups={{0,3,4,7,8,11,12,15,16,19,20,23,24,27,28,31},{1,2,5,6,9,10,13,14,17,18,..., dimensions={0}, use_global_device_ids=true | all-gather | bytes 557056 | tf_op jit(solution)/shard_map/all_gather | solution.py:511
  98.8 2.1 %collective-permute-start = (bf16[16,128,128]{2,1,0:T(8,128)(2,1)S(1)}, bf16[16,128,128]{2,1,0:T(8,128)(2,1)S(1)}, u32[]{:S(2)}, u32[]{:S(2)}) collective-permute-start(bf16[16,128,128]{2,1,0:T(8,128)(2,1)S(1)} %bitcast.38), channel_id=1, source_target_pairs={{0,1},{1,0},{2,3},{3,2},{4,5},{5,4},{6,7},{7,6},{8,9},{9,8},{10,11... | collective-permute-start | bytes 1572872 | tf_op jit(solution)/shard_map/ppermute | solution.py:512
  100.9 1.5 %own_half.1 = (f32[128,64]{1,0:T(8,128)S(1)}, f32[128,128]{1,0:T(8,128)S(1)}, bf16[4096,64]{1,0:T(8,128)(2,1)S(1)}) custom-call(s32[1]{0:T(128)} %bitcast.first_ref, bf16[16,128,128]{2,1,0:T(8,128)(2,1)S(1)} %bitcast.39, bf16[4096,64]{1,0:T(8,128)(2,1)} %bitcast.42), custom_call_target="tpu_custom_call" | custom-call | flops 33554432 | bytes 1048576 | tf_op jit(solution)/shard_map/own_half/pallas_call | solution.py:409
  102.5 0.2 collective-permute-done.pieces_ref
  102.7 0.9 last.1
  (1 shorter events, 0.0 us)
Async XLA Ops:
  0.0 47.2 %copy-start = (bf16[2048,32,2]{0,2,1:T(2,128)(2,1)S(1)}, bf16[2048,32,2]{0,2,1:T(2,128)(2,1)}, u32[]{:S(2)}) copy-start(bf16[2048,32,2]{0,2,1:T(2,128)(2,1)} %param.25) | copy-start | bytes 786436
  0.0 0.8 copy-start.2
  1.6 57.8 %all-to-all-start = ((bf16[16,64,128]{2,1,0:T(8,128)(2,1)}), bf16[16,64,128]{2,1,0:T(8,128)(2,1)S(1)}, u32[]{:S(2)}, u32[]{:S(2)}) async-start(bf16[16,64,128]{2,1,0:T(8,128)(2,1)} %pack.1), calls=%async_computation | async-start | bytes 524288 | tf_op jit(solution)/shard_map/all_to_all | solution.py:501
  50.7 16.0 %copy-start.1 = (bf16[2048,2,1,64]{0,3,2,1:T(8,128)(2,1)S(1)}, bf16[2048,2,1,64]{0,3,2,1:T(8,128)(2,1)}, u32[]{:S(2)}) copy-start(bf16[2048,2,1,64]{0,3,2,1:T(8,128)(2,1)} %param.23) | copy-start | bytes 1572868
  98.8 3.8 %collective-permute-start = (bf16[16,128,128]{2,1,0:T(8,128)(2,1)S(1)}, bf16[16,128,128]{2,1,0:T(8,128)(2,1)S(1)}, u32[]{:S(2)}, u32[]{:S(2)}) collective-permute-start(bf16[16,128,128]{2,1,0:T(8,128)(2,1)S(1)} %bitcast.38), channel_id=1, source_target_pairs={{0,1},{1,0},{2,3},{3,2},{4,5},{5,4},{6,7},{7,6},{8,9},{9,8},{10,11... | collective-permute-start | bytes 1572872 | tf_op jit(solution)/shard_map/ppermute | solution.py:512
